TPU v7x, 32 devices: a whole 2x2x4 slice. The times are simulated.
32 devices in a mesh: sp: 8 (over z, x), tp: 4 (over y, core).
Axes of the slice: x: 2, y: 2, z: 4, core: 2. Of those that a mesh axis runs over, the one named last changes fastest.
Arguments:
- residual: bfloat16 [4096, 2048], P(('sp', 'tp')), may hold values from -6 to 6
- conv_value: bfloat16 [4096, 1024], P('sp', 'tp'), may hold values from -6 to 6
- conv_gate: bfloat16 [4096, 1024], P('sp', 'tp'), may hold values from -9 to 9
- segments: int32 [4096], P('sp'), may hold values from 0 to 3, never falling along the last dimension, each value on 1 to 2048 neighbouring positions
- conv_weight: float32 [31, 1024], P(None, 'tp'), may hold values from -1 to 1
- norm_gain: float32 [1024], P('tp'), may hold values from 0.1 to 1.9
- norm_shift: float32 [1024], P('tp'), may hold values from -3 to 3
- out_weight: bfloat16 [1024, 2048], replicated, may hold values from -0.1875 to 0.1875
- ffn_gain: float32 [2048], replicated, may hold values from 0.1 to 1.9
- routes: int32 [4096, 2], P('sp'), may hold values from 0 to 7, all different within a row; in each aligned block of 128 rows (0 to 127, 128 to 255, ...) at most 64 rows name the same one
- route_weights: float32 [4096, 2], P('sp'), may hold values from 0.2 to 1
- w_gate: bfloat16 [8, 2048, 1024], P('sp', None, 'tp'), may hold values from -0.125 to 0.125
- w_up: bfloat16 [8, 2048, 1024], P('sp', None, 'tp'), may hold values from -0.125 to 0.125
- w_down: bfloat16 [8, 1024, 2048], P('sp', 'tp'), may hold values from -0.1875 to 0.1875
Outputs:
- layer_out: bfloat16 [4096, 2048], P(('sp', 'tp'))
Inputs may be any that keep to these rules, and one draw needn't show every extreme that they name: `routes`: within the rows of one device (aligned blocks of 512 / 4 rows), no expert is named more than 64 times; the two experts of a row differ. `segments`: document numbers never fall along the sequence.
All inputs are finite; a program needn't handle non-finite values.
Results may differ from a plain program's by a relative error of at most 0.007.
Values may be sent and summed in bfloat16 or wider, within the bound.
A program may use at most 128 MiB of HBM per device.

v0:
```python
import functools

import jax
import jax.numpy as jnp
from jax import lax
from jax.experimental import pallas as pl
from jax.experimental.pallas import tpu as pltpu
from jax.sharding import PartitionSpec as P

DC = 1024
CONV_GROUPS = 8
MESH = pl.DeviceIdType.MESH
RIM = 32


def passed_along(value, axis, steps):
    count = lax.axis_size(axis)
    initial, last = (max(0, -steps), min(count, count - steps))
    return lax.ppermute(value, axis, [(source, source + steps) for source in range(initial, last)])


def slot_numbers(block_routes, capacity, experts_n):
    route_pairs = block_routes.reshape(block_routes.shape[:-2] + (-1,))
    onehot = (route_pairs[..., None] == jnp.arange(experts_n, dtype=jnp.int32)).astype(jnp.int32)
    slot_rank = jnp.sum((jnp.cumsum(onehot, axis=-2) - onehot) * onehot, axis=-1)
    return (route_pairs * capacity + slot_rank).reshape(block_routes.shape)


def dispatch_matrix(slot_ids, slot_total):
    numbers = jnp.arange(slot_total, dtype=jnp.int32)[:, None, None]
    matches = jnp.any(numbers == slot_ids[..., None, :, :], axis=-1)
    return matches.astype(jnp.bfloat16)


def plain_shards(
    residual,
    conv_value,
    conv_gate,
    segments,
    conv_weight,
    norm_gain,
    norm_shift,
    out_weight,
    ffn_gain,
    routes,
    route_weights,
    w_gate,
    w_up,
    w_down,
):
    tok_dev, local_channels = conv_value.shape
    reach = conv_weight.shape[0] - 1
    whole_gate, whole_up = (
        lax.all_gather(w_gate[0], "tp", axis=1, tiled=True),
        lax.all_gather(w_up[0], "tp", axis=1, tiled=True),
    )
    whole_down = lax.all_gather(w_down[0], "tp", axis=0, tiled=True)
    gated = (conv_value.astype(jnp.float32) * jax.nn.sigmoid(conv_gate.astype(jnp.float32))).astype(
        jnp.bfloat16
    )
    rim_prev, seg_prev = passed_along(
        (gated[tok_dev - reach :], segments[tok_dev - reach :]), "sp", 1
    )
    extended = jnp.concatenate([rim_prev, gated], 0).astype(jnp.float32)
    seg_ext = jnp.concatenate([seg_prev, segments], 0)
    convolved = jnp.zeros((tok_dev, local_channels), jnp.float32)
    for offset in range(reach + 1):
        same_doc = (seg_ext[offset : offset + tok_dev] == segments)[:, None]
        convolved = convolved + jnp.where(
            same_doc, extended[offset : offset + tok_dev] * conv_weight[offset], 0.0
        )
    group_size = DC // CONV_GROUPS
    grouped = convolved.reshape(tok_dev, local_channels // group_size, group_size)
    group_mean = jnp.mean(grouped, axis=-1, keepdims=True)
    group_var = jnp.mean(jnp.square(grouped - group_mean), axis=-1, keepdims=True)
    scaled = ((grouped - group_mean) * lax.rsqrt(group_var + 1e-05)).reshape(
        tok_dev, local_channels
    ) * norm_gain + norm_shift
    conv_out = jax.nn.silu(scaled).astype(jnp.bfloat16)
    columns = lax.axis_size("tp")
    column = lax.axis_index("tp")
    rows_own = tok_dev // columns
    own_conv = lax.all_to_all(conv_out, "tp", split_axis=0, concat_axis=1, tiled=True)
    mixed = jnp.dot(own_conv, out_weight, preferred_element_type=jnp.float32)
    stream = residual.astype(jnp.float32) + lax.optimization_barrier(
        mixed.astype(jnp.bfloat16)
    ).astype(jnp.float32)
    normed = (
        stream * lax.rsqrt(jnp.mean(stream * stream, axis=-1, keepdims=True) + 1e-06) * ffn_gain
    ).astype(jnp.bfloat16)
    experts_n = lax.axis_size("sp")
    top_count = routes.shape[1]
    model_width = normed.shape[1]
    capacity = max(2, 2 * tok_dev * top_count // (columns * experts_n))
    slot_total = experts_n * capacity
    own_routes = lax.dynamic_slice_in_dim(routes, column * rows_own, rows_own, 0)
    own_weights = lax.dynamic_slice_in_dim(route_weights, column * rows_own, rows_own, 0)
    own_slots = slot_numbers(own_routes, capacity, experts_n)
    routing_table = dispatch_matrix(own_slots, slot_total)
    outgoing = jnp.dot(routing_table, normed, preferred_element_type=jnp.float32).astype(
        jnp.bfloat16
    )
    outgoing = outgoing.reshape(experts_n, capacity, model_width)
    arrived = lax.all_to_all(outgoing, "sp", split_axis=0, concat_axis=1, tiled=True).reshape(
        slot_total, model_width
    )
    gate_act = jnp.dot(arrived, whole_gate, preferred_element_type=jnp.float32)
    up_act = jnp.dot(arrived, whole_up, preferred_element_type=jnp.float32)
    hidden = (jax.nn.silu(gate_act) * up_act).astype(jnp.bfloat16)
    summed = jnp.dot(hidden, whole_down, preferred_element_type=jnp.float32)
    expert_out = summed.astype(jnp.bfloat16).reshape(experts_n, capacity, model_width)
    returned = lax.all_to_all(expert_out, "sp", split_axis=0, concat_axis=0, tiled=True).reshape(
        slot_total, model_width
    )
    combined = stream
    for member in range(top_count):
        chosen = jnp.take(returned, own_slots[:, member], axis=0).astype(jnp.float32)
        combined = combined + own_weights[:, member : member + 1] * chosen
    return combined.astype(jnp.bfloat16)


def flipped(index, mask):
    bit = 1
    while bit <= mask:
        if mask & bit:
            index = index + bit * (1 - 2 * ((index // bit) % 2))
        bit *= 2
    return index


def layer_kernel(
    experts_n, columns, capacity,
    residual_ref, value_ref, gate_ref, seg_ref, conv_w_ref, gain_ref, shift_ref, ow_hbm, ffn_ref,
    routes_ref, route_w_ref, wg_ref, wu_ref, wd_ref,
    out_ref,
    ow, wg_in, wu_in, wd_in, rim, seg_ext, ext, conv_out, conv_in, stream, normed,
    outgoing, arrived, hidden, partial, results, returned, seg_in, tables,
    ow_sem, y_send, y_recv, c_send, c_recv, f_send, f_recv, rim_send, rim_recv,
    x_send, x_recv, d_send, d_recv, r_send, r_recv,
):
    me_s, me_t = lax.axis_index("sp"), lax.axis_index("tp")
    tok_dev, local = value_ref.shape
    width = residual_ref.shape[1]
    rows_own = tok_dev // columns
    taps = conv_w_ref.shape[0]
    next_s = (me_s + 1) % experts_n
    previous_s = (me_s + experts_n - 1) % experts_n
    tile = 512

    ow_copy = pltpu.make_async_copy(ow_hbm, ow, ow_sem)
    ow_copy.start()

    def tp_peer(mask):
        return (me_s, flipped(me_t, mask))

    def sp_peer(mask):
        return (flipped(me_s, mask), me_t)

    barrier = pltpu.get_barrier_semaphore()
    peers = [tp_peer(mask) for mask in range(1, columns)]
    peers += [sp_peer(mask) for mask in range(1, experts_n)]
    for peer in peers:
        pl.semaphore_signal(barrier, inc=1, device_id=peer, device_id_type=MESH)
    pl.semaphore_wait(barrier, len(peers))

    def remote(src, dst, send, recv, peer):
        return pltpu.make_async_remote_copy(
            src_ref=src, dst_ref=dst, send_sem=send, recv_sem=recv,
            device_id=peer, device_id_type=MESH,
        )

    last = pl.ds(tok_dev - RIM, RIM)
    rim_copies = [
        remote(ref, dst, rim_send.at[i], rim_recv.at[i], (next_s, me_t))
        for i, (ref, dst) in enumerate(
            ((value_ref.at[last], rim.at[0]), (gate_ref.at[last], rim.at[1]), (seg_ref, seg_in))
        )
    ]
    for copy in rim_copies:
        copy.start()

    half = width // 2
    pieces = (
        (wg_ref, wg_in, 0, half), (wg_ref, wg_in, half, half),
        (wu_ref, wu_in, 0, width), (wd_ref, wd_in, 0, local),
    )
    across = [
        remote(own.at[pl.ds(row, n)], into.at[1, pl.ds(row, n)], y_send.at[i], y_recv.at[i], tp_peer(2))
        for i, (own, into, row, n) in enumerate(pieces)
    ]
    forward = [
        remote(into.at[1, pl.ds(row, n)], into.at[2, pl.ds(row, n)], f_send.at[i], f_recv.at[i], tp_peer(1))
        for i, (own, into, row, n) in enumerate(pieces)
    ]
    beside = [
        remote(own, into.at[0], c_send.at[i], c_recv.at[i], tp_peer(1))
        for i, (own, into) in enumerate(((wg_ref, wg_in), (wu_ref, wu_in), (wd_ref, wd_in)))
    ]
    across[0].start()

    def gated_of(value, gate):
        value, gate = value.astype(jnp.float32), gate.astype(jnp.float32)
        product = value * (1.0 / (1.0 + jnp.exp(-gate)))
        return product.astype(jnp.bfloat16).astype(jnp.float32)

    def gate_rows(i, carry):
        row = pl.multiple_of(i * 64, 64)
        ext[pl.ds(row + RIM, 64), :] = gated_of(value_ref[pl.ds(row, 64), :], gate_ref[pl.ds(row, 64), :])
        return carry

    lax.fori_loop(0, tok_dev // 64, gate_rows, 0)
    lanes_n = seg_ref.shape[1]

    def column(row):
        return jnp.broadcast_to(row.astype(jnp.float32), (lanes_n, lanes_n)).T

    for i in range(seg_ref.shape[0]):
        seg_ext[RIM + i * lanes_n : RIM + (i + 1) * lanes_n, :] = column(seg_ref[i : i + 1, :])
    own_lanes = pl.ds(pl.multiple_of(me_t * rows_own, rows_own), rows_own)
    numbers = lax.broadcasted_iota(jnp.int32, (rows_own, lanes_n), 1).astype(jnp.float32)
    names = [column(routes_ref[m : m + 1, own_lanes]) for m in range(routes_ref.shape[0])]
    shares = [column(route_w_ref[m : m + 1, own_lanes])[:, 0:1] for m in range(routes_ref.shape[0])]
    marks = [jnp.where(name == numbers, 1.0, 0.0) for name in names]
    earlier = jnp.where(
        lax.broadcasted_iota(jnp.int32, (rows_own, rows_own), 0)
        > lax.broadcasted_iota(jnp.int32, (rows_own, rows_own), 1), 1.0, 0.0,
    ).astype(jnp.bfloat16)
    counts = jnp.dot(earlier, sum(marks).astype(jnp.bfloat16), preferred_element_type=jnp.float32)
    slot_places = lax.broadcasted_iota(jnp.int32, (rows_own, experts_n * capacity), 1)
    for m, mark in enumerate(marks):
        rank = jnp.sum(counts * mark, axis=-1, keepdims=True).astype(jnp.int32)
        slot = (names[m][:, 0:1].astype(jnp.int32) ^ me_s) * capacity + rank
        tables[m] = jnp.where(slot_places == slot, 1.0, 0.0).astype(jnp.bfloat16)
    for copy in rim_copies:
        copy.wait_recv()
    ext[pl.ds(0, RIM), :] = gated_of(rim[0], rim[1])
    before = column(seg_in[seg_ref.shape[0] - 1 : seg_ref.shape[0], :])[lanes_n - RIM :, :]
    seg_ext[0:RIM, :] = jnp.where(me_s == 0, -1.0, before)

    group = DC // CONV_GROUPS
    block = 64
    lead = RIM - (taps - 1)
    for row in range(0, tok_dev, block):
        own_seg = seg_ext[row + RIM : row + RIM + block, :]
        sums = [jnp.zeros((block, group), jnp.float32) for _ in range(local // group)]
        for tap in range(taps):
            at = row + lead + tap
            same_doc = seg_ext[at : at + block, :] == own_seg
            for g in range(local // group):
                lanes = slice(g * group, (g + 1) * group)
                term = ext[at : at + block, lanes] * conv_w_ref[tap : tap + 1, lanes]
                sums[g] = sums[g] + jnp.where(same_doc, term, 0.0)
        for g in range(local // group):
            lanes = slice(g * group, (g + 1) * group)
            mean = jnp.mean(sums[g], axis=-1, keepdims=True)
            centred = sums[g] - mean
            deviation = jnp.mean(centred * centred, axis=-1, keepdims=True)
            scaled = centred * lax.rsqrt(deviation + 1e-05) * gain_ref[:, lanes] + shift_ref[:, lanes]
            conv_out[row : row + block, lanes] = (scaled / (1.0 + jnp.exp(-scaled))).astype(jnp.bfloat16)

    exchange = {}
    for mask in (3, 2, 1):
        peer_rows = pl.ds(pl.multiple_of(flipped(me_t, mask) * rows_own, rows_own), rows_own)
        exchange[mask] = remote(
            conv_out.at[peer_rows], conv_in.at[mask], x_send.at[mask], x_recv.at[mask], tp_peer(mask)
        )
        exchange[mask].start()
    for copy in across[1:] + beside:
        copy.start()
    conv_in[0] = conv_out[pl.ds(pl.multiple_of(me_t * rows_own, rows_own), rows_own), :]
    ow_copy.wait()
    for mask in (1, 2, 3):
        exchange[mask].wait_recv()

    squares = jnp.zeros((rows_own, 1), jnp.float32)
    for col in range(0, width, tile):
        cols = slice(col, col + tile)
        mixed = jnp.zeros((rows_own, tile), jnp.float32)
        for mask in range(columns):
            w_rows = pl.ds(pl.multiple_of(flipped(me_t, mask) * local, local), local)
            mixed = mixed + jnp.dot(conv_in[mask], ow[w_rows, cols], preferred_element_type=jnp.float32)
        part = residual_ref[:, cols].astype(jnp.float32) + mixed.astype(jnp.bfloat16).astype(jnp.float32)
        stream[:, cols] = part
        squares = squares + jnp.sum(part * part, axis=-1, keepdims=True)
    scale = lax.rsqrt(squares / width + 1e-06)
    normed[...] = (stream[...] * scale * ffn_ref[...]).astype(jnp.bfloat16)

    dispatch = [
        None if mask == 0 else remote(
            outgoing.at[pl.ds(mask * capacity, capacity)], arrived.at[pl.ds(mask * capacity, capacity)],
            d_send.at[mask], d_recv.at[mask], sp_peer(mask),
        )
        for mask in range(experts_n)
    ]
    half_slots = experts_n * capacity // 2
    for part in (1, 0):
        first = part * half_slots
        picks = sum(
            tables[m, :, first : first + half_slots].astype(jnp.float32) for m in range(len(names))
        ).T.astype(jnp.bfloat16)
        for col in range(0, width, tile):
            cols = slice(col, col + tile)
            outgoing[first : first + half_slots, cols] = jnp.dot(
                picks, normed[:, cols], preferred_element_type=jnp.float32
            ).astype(jnp.bfloat16)
        for mask in reversed(range(part * experts_n // 2, (part + 1) * experts_n // 2)):
            if mask:
                dispatch[mask].start()
    arrived[0:capacity, :] = outgoing[0:capacity, :]

    near, far = slice(0, half_slots), slice(half_slots, 2 * half_slots)

    def hidden_units(mask, rows):
        g = wg_ref[...] if mask == 0 else wg_in[mask - 1]
        u = wu_ref[...] if mask == 0 else wu_in[mask - 1]
        gate_act = jnp.dot(arrived[rows, :], g, preferred_element_type=jnp.float32)
        up_act = jnp.dot(arrived[rows, :], u, preferred_element_type=jnp.float32)
        hidden[mask, rows, :] = (gate_act / (1.0 + jnp.exp(-gate_act)) * up_act).astype(jnp.bfloat16)

    for copy in beside:
        copy.wait_recv()
    for i in (0, 1):
        across[i].wait_recv()
        forward[i].start()
    for mask in range(1, experts_n // 2):
        dispatch[mask].wait_recv()
    hidden_units(0, near)
    hidden_units(1, near)
    across[2].wait_recv()
    forward[2].start()
    hidden_units(2, near)
    for i in (0, 1, 2):
        forward[i].wait_recv()
    hidden_units(3, near)
    for mask in range(experts_n // 2, experts_n):
        dispatch[mask].wait_recv()
    for mask in range(columns):
        hidden_units(mask, far)
    def down(mask, rows, cols):
        w = wd_ref[:, cols] if mask == 0 else wd_in[mask - 1, :, cols]
        return jnp.dot(hidden[mask, rows, :], w, preferred_element_type=jnp.float32)

    for rows in (far, near):
        for col in range(0, width, tile):
            cols = slice(col, col + tile)
            partial[rows, cols] = down(0, rows, cols) + down(1, rows, cols)
    across[3].wait_recv()
    forward[3].start()
    for col in range(0, width, tile):
        cols = slice(col, col + tile)
        partial[far, cols] += down(2, far, cols)
    forward[3].wait_recv()

    give_back = [
        None if mask == 0 else remote(
            results.at[pl.ds(mask * capacity, capacity)], returned.at[pl.ds(mask * capacity, capacity)],
            r_send.at[mask], r_recv.at[mask], sp_peer(mask),
        )
        for mask in range(experts_n)
    ]
    for part in (1, 0):
        rows = (near, far)[part]
        for col in range(0, width, tile):
            cols = slice(col, col + tile)
            total = partial[rows, cols] + down(3, rows, cols)
            if part == 0:
                total = total + down(2, rows, cols)
            results[rows, cols] = total.astype(jnp.bfloat16)
        for mask in reversed(range(part * experts_n // 2, (part + 1) * experts_n // 2)):
            if mask:
                give_back[mask].start()
    returned[0:capacity, :] = results[0:capacity, :]

    for part in (0, 1):
        rows = (near, far)[part]
        for mask in range(part * experts_n // 2, (part + 1) * experts_n // 2):
            if mask:
                give_back[mask].wait_recv()
        for col in range(0, width, tile):
            cols = slice(col, col + tile)
            total = stream[:, cols]
            for m, share in enumerate(shares):
                chosen = jnp.dot(tables[m, :, rows], returned[rows, cols], preferred_element_type=jnp.float32)
                total = total + share * chosen
            if part == 0:
                stream[:, cols] = total
            else:
                out_ref[:, cols] = total.astype(jnp.bfloat16)

    for copy in rim_copies + across + forward + beside + list(exchange.values()):
        copy.wait_send()
    for mask in range(1, experts_n):
        dispatch[mask].wait_send()
        give_back[mask].wait_send()


def shards(*args):
    (residual, conv_value, conv_gate, segments, conv_weight, norm_gain, norm_shift, out_weight,
     ffn_gain, routes, route_weights, w_gate, w_up, w_down) = args
    tok_dev, local = conv_value.shape
    width = residual.shape[1]
    experts_n, columns = lax.axis_size("sp"), lax.axis_size("tp")
    top_count = routes.shape[1]
    capacity = max(2, 2 * tok_dev * top_count // (columns * experts_n))
    if capacity % 32 or columns != 4 or tok_dev != columns * 128 or experts_n & (experts_n - 1):
        return plain_shards(*args)
    rows_own = tok_dev // columns
    lanes = DC // CONV_GROUPS
    slot_total = experts_n * capacity
    bf16, f32 = jnp.bfloat16, jnp.float32
    vmem, dma = pltpu.VMEM, pltpu.SemaphoreType.DMA
    spec = pl.BlockSpec(memory_space=pltpu.VMEM)
    specs = [spec] * 14
    specs[7] = pl.BlockSpec(memory_space=pl.ANY)
    return pl.pallas_call(
        functools.partial(layer_kernel, experts_n, columns, capacity),
        out_shape=jax.ShapeDtypeStruct((rows_own, width), bf16),
        in_specs=specs,
        out_specs=spec,
        scratch_shapes=[
            vmem(out_weight.shape, bf16),
            vmem((3, width, local), bf16), vmem((3, width, local), bf16), vmem((3, local, width), bf16),
            vmem((2, RIM, local), bf16), vmem((RIM + tok_dev, lanes), f32),
            vmem((RIM + tok_dev, local), f32), vmem((tok_dev, local), bf16),
            vmem((columns, rows_own, local), bf16), vmem((rows_own, width), f32),
            vmem((rows_own, width), bf16), vmem((slot_total, width), bf16),
            vmem((slot_total, width), bf16), vmem((columns, slot_total, local), bf16),
            vmem((slot_total, width), f32),
            vmem((slot_total, width), bf16), vmem((slot_total, width), bf16),
            vmem((tok_dev // lanes, lanes), jnp.int32), vmem((top_count, rows_own, slot_total), bf16),
            dma, dma((4,)), dma((4,)), dma((3,)), dma((3,)), dma((4,)), dma((4,)), dma((3,)), dma((3,)),
            dma((4,)), dma((4,)), dma((experts_n,)), dma((experts_n,)), dma((experts_n,)), dma((experts_n,)),
        ],
        compiler_params=pltpu.CompilerParams(
            collective_id=0, has_side_effects=True, vmem_limit_bytes=60 * 1024 * 1024
        ),
    )(
        residual, conv_value, conv_gate,
        segments.reshape(-1, lanes), conv_weight,
        norm_gain[None], norm_shift[None], out_weight, ffn_gain[None],
        routes.T, route_weights.T, w_gate[0], w_up[0], w_down[0],
    )


def solution(mesh):
    return jax.shard_map(
        shards,
        mesh=mesh,
        in_specs=(
            P(("sp", "tp"), None),
            P("sp", "tp"),
            P("sp", "tp"),
            P("sp"),
            P(None, "tp"),
            P("tp"),
            P("tp"),
            P(),
            P(),
            P("sp", None),
            P("sp", None),
            P("sp", None, "tp"),
            P("sp", None, "tp"),
            P("sp", "tp", None),
        ),
        out_specs=P(("sp", "tp"), None),
        check_vma=False,
    )
```

profile of v0, /device:TPU:0, one launch (start us, length us, event | category | flops | bytes accessed | tf_op | source)
XLA Modules:
  0.0 136.0 jit_solution(12966938608821017847)
XLA Ops:
  0.0 134.1 %shard_map.136 = bf16[128,2048]{1,0:T(8,128)(2,1)} custom-call(bf16[128,2048]{1,0:T(8,128)(2,1)} %residual_ref.1, bf16[512,256]{1,0:T(8,128)(2,1)} %value_ref.1, bf16[512,256]{1,0:T(8,128)(2,1)} %gate_ref.1, s32[4,128]{1,0:T(4,128)} %bitcast.15, f32[31,256]{1,0:T(8,128)} %conv_w_ref.1, f32[1,256]{1,0:T(1,128)} %bitcast.16, f32[1,256]{1,0:T(1,128)} %bitcast.17, ...), custom_call_target="tpu_custom_call" | custom-call | tf_op jit(solution)/shard_map/pallas_call | solution.py:415
  134.1 1.9 %copy.16 = bf16[128,2048]{1,0:T(8,128)(2,1)} copy(bf16[128,2048]{1,0:T(8,128)(2,1)} %shard_map.136) | data formatting | bytes 1048576
where the time goes:
time: 136 us
  Pallas kernels  134 us (99%)
  local copies, waits for them, and re-layouts  1.88 us (1%)
    pallas_call x1, Pallas kernels, shards(): pl.pallas_call(functools.partial(layer_kernel, experts_n, columns, capaci...  134 us

commit v1 on v0

v1 whole, which is shorter than its diff:
```python
import functools

import jax
import jax.numpy as jnp
from jax import lax
from jax.experimental import pallas as pl
from jax.experimental.pallas import tpu as pltpu
from jax.sharding import PartitionSpec as P

DC = 1024
CONV_GROUPS = 8
MESH = pl.DeviceIdType.MESH
RIM = 32


def passed_along(value, axis, steps):
    count = lax.axis_size(axis)
    initial, last = (max(0, -steps), min(count, count - steps))
    return lax.ppermute(value, axis, [(source, source + steps) for source in range(initial, last)])


def slot_numbers(block_routes, capacity, experts_n):
    route_pairs = block_routes.reshape(block_routes.shape[:-2] + (-1,))
    onehot = (route_pairs[..., None] == jnp.arange(experts_n, dtype=jnp.int32)).astype(jnp.int32)
    slot_rank = jnp.sum((jnp.cumsum(onehot, axis=-2) - onehot) * onehot, axis=-1)
    return (route_pairs * capacity + slot_rank).reshape(block_routes.shape)


def dispatch_matrix(slot_ids, slot_total):
    numbers = jnp.arange(slot_total, dtype=jnp.int32)[:, None, None]
    matches = jnp.any(numbers == slot_ids[..., None, :, :], axis=-1)
    return matches.astype(jnp.bfloat16)


def plain_shards(
    residual,
    conv_value,
    conv_gate,
    segments,
    conv_weight,
    norm_gain,
    norm_shift,
    out_weight,
    ffn_gain,
    routes,
    route_weights,
    w_gate,
    w_up,
    w_down,
):
    tok_dev, local_channels = conv_value.shape
    reach = conv_weight.shape[0] - 1
    whole_gate, whole_up = (
        lax.all_gather(w_gate[0], "tp", axis=1, tiled=True),
        lax.all_gather(w_up[0], "tp", axis=1, tiled=True),
    )
    whole_down = lax.all_gather(w_down[0], "tp", axis=0, tiled=True)
    gated = (conv_value.astype(jnp.float32) * jax.nn.sigmoid(conv_gate.astype(jnp.float32))).astype(
        jnp.bfloat16
    )
    rim_prev, seg_prev = passed_along(
        (gated[tok_dev - reach :], segments[tok_dev - reach :]), "sp", 1
    )
    extended = jnp.concatenate([rim_prev, gated], 0).astype(jnp.float32)
    seg_ext = jnp.concatenate([seg_prev, segments], 0)
    convolved = jnp.zeros((tok_dev, local_channels), jnp.float32)
    for offset in range(reach + 1):
        same_doc = (seg_ext[offset : offset + tok_dev] == segments)[:, None]
        convolved = convolved + jnp.where(
            same_doc, extended[offset : offset + tok_dev] * conv_weight[offset], 0.0
        )
    group_size = DC // CONV_GROUPS
    grouped = convolved.reshape(tok_dev, local_channels // group_size, group_size)
    group_mean = jnp.mean(grouped, axis=-1, keepdims=True)
    group_var = jnp.mean(jnp.square(grouped - group_mean), axis=-1, keepdims=True)
    scaled = ((grouped - group_mean) * lax.rsqrt(group_var + 1e-05)).reshape(
        tok_dev, local_channels
    ) * norm_gain + norm_shift
    conv_out = jax.nn.silu(scaled).astype(jnp.bfloat16)
    columns = lax.axis_size("tp")
    column = lax.axis_index("tp")
    rows_own = tok_dev // columns
    own_conv = lax.all_to_all(conv_out, "tp", split_axis=0, concat_axis=1, tiled=True)
    mixed = jnp.dot(own_conv, out_weight, preferred_element_type=jnp.float32)
    stream = residual.astype(jnp.float32) + lax.optimization_barrier(
        mixed.astype(jnp.bfloat16)
    ).astype(jnp.float32)
    normed = (
        stream * lax.rsqrt(jnp.mean(stream * stream, axis=-1, keepdims=True) + 1e-06) * ffn_gain
    ).astype(jnp.bfloat16)
    experts_n = lax.axis_size("sp")
    top_count = routes.shape[1]
    model_width = normed.shape[1]
    capacity = max(2, 2 * tok_dev * top_count // (columns * experts_n))
    slot_total = experts_n * capacity
    own_routes = lax.dynamic_slice_in_dim(routes, column * rows_own, rows_own, 0)
    own_weights = lax.dynamic_slice_in_dim(route_weights, column * rows_own, rows_own, 0)
    own_slots = slot_numbers(own_routes, capacity, experts_n)
    routing_table = dispatch_matrix(own_slots, slot_total)
    outgoing = jnp.dot(routing_table, normed, preferred_element_type=jnp.float32).astype(
        jnp.bfloat16
    )
    outgoing = outgoing.reshape(experts_n, capacity, model_width)
    arrived = lax.all_to_all(outgoing, "sp", split_axis=0, concat_axis=1, tiled=True).reshape(
        slot_total, model_width
    )
    gate_act = jnp.dot(arrived, whole_gate, preferred_element_type=jnp.float32)
    up_act = jnp.dot(arrived, whole_up, preferred_element_type=jnp.float32)
    hidden = (jax.nn.silu(gate_act) * up_act).astype(jnp.bfloat16)
    summed = jnp.dot(hidden, whole_down, preferred_element_type=jnp.float32)
    expert_out = summed.astype(jnp.bfloat16).reshape(experts_n, capacity, model_width)
    returned = lax.all_to_all(expert_out, "sp", split_axis=0, concat_axis=0, tiled=True).reshape(
        slot_total, model_width
    )
    combined = stream
    for member in range(top_count):
        chosen = jnp.take(returned, own_slots[:, member], axis=0).astype(jnp.float32)
        combined = combined + own_weights[:, member : member + 1] * chosen
    return combined.astype(jnp.bfloat16)


def flipped(index, mask):
    bit = 1
    while bit <= mask:
        if mask & bit:
            index = index + bit * (1 - 2 * ((index // bit) % 2))
        bit *= 2
    return index


def layer_kernel(
    experts_n, columns, capacity, blocks,
    residual_hbm, value_hbm, gate_hbm, seg_ref, conv_w_ref, gain_ref, shift_ref, ow_hbm, ffn_ref,
    routes_ref, route_w_ref, wg_hbm, wu_hbm, wd_hbm,
    out_ref,
    residual, value, gate, ow, wg, wu, wd, wg_in, wu_in, wd_in, rim, seg_in, seg_ext, ext, win, seg_win,
    conv_out, conv_in, stream, normed, outgoing, arrived, rows_in, relay_out, hidden, partial,
    results, returned, relay_in, relay_sum, far_in, tables, picks, shares, routes_in, route_w_in,
    load_sem, y_send, y_recv, c_send, c_recv, f_send, f_recv, rim_send, rim_recv, x_send, x_recv,
    t_send, t_recv, far_send, far_recv, d_send, d_recv, rd_send,
    rb_send, rb_recv, r_send, r_recv, sum_send, sum_recv,
):
    me_s, me_t = lax.axis_index("sp"), lax.axis_index("tp")
    tok_dev, local = value.shape
    width = residual.shape[1]
    rows_own = tok_dev // columns
    taps = conv_w_ref.shape[0]
    halves = normed.shape[0]
    half = width // halves
    band = width // blocks
    near_n = experts_n // 2
    near_slots = near_n * capacity
    next_s = (me_s + 1) % experts_n
    tile = 512
    group = DC // CONV_GROUPS
    level = me_s // 2
    levels = experts_n // 2
    in_middle = jnp.logical_or(level == levels // 2 - 1, level == levels // 2)
    at_end = jnp.logical_not(in_middle)

    def tp_peer(mask):
        return (me_s, flipped(me_t, mask))

    def sp_peer(mask):
        return (flipped(me_s, mask), me_t)

    loads = [
        pltpu.make_async_copy(src, dst, load_sem.at[i])
        for i, (src, dst) in enumerate((
            (value_hbm, value), (gate_hbm, gate), (residual_hbm, residual), (ow_hbm, ow),
            (wg_hbm, wg), (wu_hbm, wu), (wd_hbm, wd),
        ))
    ]
    barrier = pltpu.get_barrier_semaphore()
    peers = [tp_peer(mask) for mask in range(1, columns)]
    peers += [sp_peer(mask) for mask in range(1, experts_n)]
    for peer in peers:
        pl.semaphore_signal(barrier, inc=1, device_id=peer, device_id_type=MESH)
    for load in loads:
        load.start()
    pl.semaphore_wait(barrier, len(peers))

    def remote(src, dst, send, recv, peer):
        return pltpu.make_async_remote_copy(
            src_ref=src, dst_ref=dst, send_sem=send, recv_sem=recv,
            device_id=peer, device_id_type=MESH,
        )

    last = pl.ds(tok_dev - RIM, RIM)
    rim_copies = [
        remote(ref, dst, rim_send.at[i], rim_recv.at[i], (next_s, me_t))
        for i, (ref, dst) in enumerate(
            ((value_hbm.at[last], rim.at[0]), (gate_hbm.at[last], rim.at[1]), (seg_ref, seg_in))
        )
    ]
    for copy in rim_copies:
        copy.start()

    def across_piece(i, own, into, rows, cols):
        return (
            remote(own.at[rows, cols], into.at[1, rows, cols], y_send.at[i], y_recv.at[i], tp_peer(2)),
            remote(into.at[1, rows, cols], into.at[2, rows, cols], f_send.at[i], f_recv.at[i], tp_peer(1)),
        )

    every, first_rows = pl.ds(0, local), width // 4
    pieces = [
        (wg_hbm, wg_in, pl.ds(0, first_rows), every),
        (wg_hbm, wg_in, pl.ds(first_rows, width - first_rows), every),
        (wu_hbm, wu_in, pl.ds(0, width // 2), every),
        (wu_hbm, wu_in, pl.ds(width // 2, width // 2), every),
    ]
    up_done = len(pieces)
    pieces += [(wd_hbm, wd_in, every, pl.ds(j * band, band)) for j in range(blocks)]
    across, forward = zip(*[across_piece(i, *piece) for i, piece in enumerate(pieces)])
    beside = [
        remote(own, into.at[0], c_send.at[i], c_recv.at[i], tp_peer(1))
        for i, (own, into) in enumerate(((wg_hbm, wg_in), (wu_hbm, wu_in), (wd_hbm, wd_in)))
    ]
    across[0].start()

    relay = jnp.where(in_middle, flipped(me_s, 6), flipped(me_s, 4))
    relay_slot = jnp.where(in_middle, 0, 1)
    route_copies = [
        remote(ref, dst.at[relay_slot], t_send.at[i], t_recv.at[relay_slot, i], (relay, me_t))
        for i, (ref, dst) in enumerate(((routes_ref, routes_in), (route_w_ref, route_w_in)))
    ]
    for copy in route_copies:
        copy.start()

    def gated_of(v, g):
        v, g = v.astype(jnp.float32), g.astype(jnp.float32)
        product = v * (1.0 / (1.0 + jnp.exp(-g)))
        return product.astype(jnp.bfloat16).astype(jnp.float32)

    def gate_rows(i, carry):
        row = pl.multiple_of(i * 64, 64)
        ext[pl.ds(row + RIM, 64), :] = gated_of(value[pl.ds(row, 64), :], gate[pl.ds(row, 64), :])
        return carry

    for load in loads[:2]:
        load.wait()
    lax.fori_loop(0, tok_dev // 64, gate_rows, 0)
    lanes_n = seg_ref.shape[1]

    def column(row):
        return jnp.broadcast_to(row.astype(jnp.float32), (lanes_n, lanes_n)).T

    for i in range(seg_ref.shape[0]):
        seg_ext[RIM + i * lanes_n : RIM + (i + 1) * lanes_n, :] = column(seg_ref[i : i + 1, :])

    for copy in rim_copies:
        copy.wait_recv()
    ext[pl.ds(0, RIM), :] = gated_of(rim[0], rim[1])
    before = column(seg_in[seg_ref.shape[0] - 1 : seg_ref.shape[0], :])[lanes_n - RIM :, :]
    seg_ext[0:RIM, :] = jnp.where(me_s == 0, -1.0, before)

    block = 64
    lead = RIM - (taps - 1)

    def conv_rows(row):
        win[...] = ext[pl.ds(row, RIM + block), :]
        seg_win[...] = seg_ext[pl.ds(row, RIM + block), :]
        own_seg = seg_win[RIM:, :]
        sums = [jnp.zeros((block, group), jnp.float32) for _ in range(local // group)]
        for tap in range(taps):
            at = lead + tap
            same_doc = seg_win[at : at + block, :] == own_seg
            for g in range(local // group):
                lanes = slice(g * group, (g + 1) * group)
                term = win[at : at + block, lanes] * conv_w_ref[tap : tap + 1, lanes]
                sums[g] = sums[g] + jnp.where(same_doc, term, 0.0)
        for g in range(local // group):
            lanes = slice(g * group, (g + 1) * group)
            mean = jnp.mean(sums[g], axis=-1, keepdims=True)
            centred = sums[g] - mean
            deviation = jnp.mean(centred * centred, axis=-1, keepdims=True)
            scaled = centred * lax.rsqrt(deviation + 1e-05) * gain_ref[:, lanes] + shift_ref[:, lanes]
            conv_out[pl.ds(row, block), lanes] = (scaled / (1.0 + jnp.exp(-scaled))).astype(jnp.bfloat16)

    exchange = {}
    for mask in (3, 2, 1, 0):
        peer_row = pl.multiple_of(flipped(me_t, mask) * rows_own, rows_own)

        def conv_step(i, carry):
            conv_rows(pl.multiple_of(peer_row + i * block, block))
            return carry

        lax.fori_loop(0, rows_own // block, conv_step, 0)
        if mask:
            exchange[mask] = remote(
                conv_out.at[pl.ds(peer_row, rows_own)], conv_in.at[mask],
                x_send.at[mask], x_recv.at[mask], tp_peer(mask),
            )
            exchange[mask].start()
        else:
            conv_in[0] = conv_out[pl.ds(peer_row, rows_own), :]
        if mask == 2:
            for copy in across[1:]:
                copy.start()

    for copy in beside:
        copy.start()
    numbers = lax.broadcasted_iota(jnp.int32, (rows_own, lanes_n), 1).astype(jnp.float32)
    earlier = jnp.where(
        lax.broadcasted_iota(jnp.int32, (rows_own, rows_own), 0)
        > lax.broadcasted_iota(jnp.int32, (rows_own, rows_own), 1), 1.0, 0.0,
    ).astype(jnp.bfloat16)
    slot_places = lax.broadcasted_iota(jnp.int32, (rows_own, near_slots), 1)
    own_lanes = pl.ds(pl.multiple_of(me_t * rows_own, rows_own), rows_own)
    top_count = routes_ref.shape[0]

    def make_tables(which, route_row, weight_row):
        names = [column(route_row(m)) for m in range(top_count)]
        marks = [jnp.where(name == numbers, 1.0, 0.0) for name in names]
        counts = jnp.dot(earlier, sum(marks).astype(jnp.bfloat16), preferred_element_type=jnp.float32)
        total = jnp.zeros((rows_own, near_slots), jnp.float32)
        for m, mark in enumerate(marks):
            rank = jnp.sum(counts * mark, axis=-1, keepdims=True).astype(jnp.int32)
            slot = (names[m][:, 0:1].astype(jnp.int32) ^ me_s) * capacity + rank
            table = jnp.where(slot_places == slot, 1.0, 0.0)
            tables[which, m] = table.astype(jnp.bfloat16)
            total = total + table
            shares[which, m] = column(weight_row(m))
        picks[which] = total.T.astype(jnp.bfloat16)

    make_tables(
        0, lambda m: routes_ref[m : m + 1, own_lanes], lambda m: route_w_ref[m : m + 1, own_lanes]
    )

    @pl.when(in_middle)
    def _():
        for slot in range(2):
            for i, ref in enumerate((routes_ref, route_w_ref)):
                dst = (routes_in, route_w_in)[i].at[slot]
                remote(ref, dst, t_send.at[i], t_recv.at[slot, i], (relay, me_t)).wait_recv()
            make_tables(
                1 + slot,
                lambda m: routes_in[slot, m : m + 1, own_lanes],
                lambda m: route_w_in[slot, m : m + 1, own_lanes],
            )

    across[0].wait_recv()
    forward[0].start()
    for load in loads[2:4]:
        load.wait()
    for mask in (1, 2, 3):
        exchange[mask].wait_recv()

    squares = jnp.zeros((rows_own, 1), jnp.float32)
    for col in range(0, width, tile):
        cols = slice(col, col + tile)
        mixed = jnp.zeros((rows_own, tile), jnp.float32)
        for mask in range(columns):
            w_rows = pl.ds(pl.multiple_of(flipped(me_t, mask) * local, local), local)
            mixed = mixed + jnp.dot(conv_in[mask], ow[w_rows, cols], preferred_element_type=jnp.float32)
        part = residual[:, cols].astype(jnp.float32) + mixed.astype(jnp.bfloat16).astype(jnp.float32)
        stream[:, cols] = part
        squares = squares + jnp.sum(part * part, axis=-1, keepdims=True)
    scale = lax.rsqrt(squares / width + 1e-06)
    far_rows = []
    for h in range(halves):
        cols = slice(h * half, (h + 1) * half)
        normed[h] = (stream[:, cols] * scale * ffn_ref[:, cols]).astype(jnp.bfloat16)
        far_rows.append(remote(
            normed.at[h], rows_in.at[relay_slot, h], far_send.at[h], far_recv.at[relay_slot, h], (relay, me_t)
        ))
        far_rows[h].start()

    def packet(mask):
        return pl.ds(mask * capacity, capacity)

    dispatch = {}
    for h in range(halves):
        for col in range(0, half, tile):
            cols = slice(col, col + tile)
            outgoing[h, :, cols] = jnp.dot(
                picks[0], normed[h, :, cols], preferred_element_type=jnp.float32
            ).astype(jnp.bfloat16)
        for mask in range(near_n - 1, 0, -1):
            dispatch[mask, h] = remote(
                outgoing.at[h, packet(mask)], arrived.at[h, packet(mask)],
                d_send.at[mask, h], d_recv.at[mask, h], sp_peer(mask),
            )
            dispatch[mask, h].start()
        arrived[h, 0:capacity, :] = outgoing[h, 0:capacity, :]

    relay_masks = ((6, 7, 4, 5), (4, 5, 6, 7))

    def relayed(slot, m, h):
        return remote(
            relay_out.at[slot, h, packet(m)], arrived.at[h, packet(relay_masks[slot][m])],
            rd_send.at[slot, m, h], d_recv.at[relay_masks[slot][m], h], sp_peer(m),
        )

    def relay_half(h):
        @pl.when(in_middle)
        def _():
            for slot in range(2):
                remote(
                    normed.at[h], rows_in.at[slot, h], far_send.at[h], far_recv.at[slot, h], (relay, me_t)
                ).wait_recv()
                for col in range(0, half, tile):
                    cols = slice(col, col + tile)
                    relay_out[slot, h, :, cols] = jnp.dot(
                        picks[1 + slot], rows_in[slot, h, :, cols], preferred_element_type=jnp.float32
                    ).astype(jnp.bfloat16)
                for m in (2, 3, 1):
                    relayed(slot, m, h).start()
                place = relay_masks[slot][0] * capacity
                arrived[h, place : place + capacity, :] = relay_out[slot, h, 0:capacity, :]

    def d_wait(mask, h):
        remote(
            outgoing.at[h, packet(0)], arrived.at[h, packet(mask)],
            d_send.at[0, h], d_recv.at[mask, h], sp_peer(1),
        ).wait_recv()

    relay_half(0)

    for load in loads[4:]:
        load.wait()
    for copy in beside:
        copy.wait_recv()
    across[1].wait_recv()
    forward[1].start()

    for h in range(1, halves):
        relay_half(h)

    for h in range(halves):
        for mask in range(1, near_n):
            d_wait(mask, h)

    near, far = slice(0, near_slots), slice(near_slots, 2 * near_slots)
    whole = slice(0, 2 * near_slots)

    def hidden_units(mask, rows):
        g = wg if mask == 0 else wg_in.at[mask - 1]
        u = wu if mask == 0 else wu_in.at[mask - 1]

        def act(w):
            return sum(
                jnp.dot(arrived[h, rows, :], w[h * half : (h + 1) * half, :], preferred_element_type=jnp.float32)
                for h in range(halves)
            )

        gate_act, up_act = act(g), act(u)
        hidden[mask, rows, :] = (gate_act / (1.0 + jnp.exp(-gate_act)) * up_act).astype(jnp.bfloat16)

    hidden_units(0, near)
    hidden_units(1, near)

    across[2].wait_recv()
    forward[2].start()

    for h in range(halves):
        for mask in range(near_n + 1, experts_n, 2):
            d_wait(mask, h)

    @pl.when(at_end)
    def _():
        for h in range(halves):
            for mask in range(near_n, experts_n, 2):
                d_wait(mask, h)

    hidden_units(0, far)
    hidden_units(1, far)

    across[3].wait_recv()
    forward[3].start()

    hidden_units(2, whole)

    for i in range(up_done):
        forward[i].wait_recv()

    hidden_units(3, whole)

    def to_relay(mask, m, slot, j):
        return remote(
            results.at[j, packet(mask)], relay_in.at[slot, j, packet(m)],
            rb_send.at[mask, j], rb_recv.at[slot, m, j], sp_peer(m),
        )

    from_middle = ((7, 1, 0), (5, 1, 1))
    from_end = ((4, 2, 0), (6, 2, 1), (5, 3, 0), (7, 3, 1))
    kept = ((6, 0), (4, 1))
    give_back = {
        (mask, j): remote(
            results.at[j, packet(mask)], returned.at[j, packet(mask)],
            r_send.at[mask, j], r_recv.at[mask, j], sp_peer(mask),
        )
        for j in range(blocks) for mask in range(1, near_n)
    }

    def band_results(j):
        cols = slice(j * band, (j + 1) * band)
        across[up_done + j].wait_recv()
        forward[up_done + j].start()

        def down(mask):
            w = wd[:, cols] if mask == 0 else wd_in[mask - 1, :, cols]
            return jnp.dot(hidden[mask], w, preferred_element_type=jnp.float32)

        partial[...] = down(0) + down(1) + down(2)
        forward[up_done + j].wait_recv()
        results[j] = (partial[...] + down(3)).astype(jnp.bfloat16)

        @pl.when(in_middle)
        def _():
            for mask, m, slot in from_middle:
                to_relay(mask, m, slot, j).start()
            for mask, slot in kept:
                relay_in[slot, j, 0:capacity, :] = results[j, mask * capacity : (mask + 1) * capacity, :]

        @pl.when(at_end)
        def _():
            for mask, m, slot in from_end:
                to_relay(mask, m, slot, j).start()

        returned[j, 0:capacity, :] = results[j, 0:capacity, :]

    def direct(j):
        for mask in range(near_n - 1, 0, -1):
            give_back[mask, j].start()

    def summed_up(slot, j):
        return remote(
            relay_sum.at[slot, j], far_in.at[j], sum_send.at[slot, j], sum_recv.at[j],
            sp_peer((6, 4)[slot]),
        )

    def weighed(which, packets):
        return sum(
            shares[which, m][:, 0:1] * jnp.dot(tables[which, m], packets, preferred_element_type=jnp.float32)
            for m in range(top_count)
        )

    def relay_band(j):
        @pl.when(in_middle)
        def _():
            for slot in range(2):
                for m in range(1, near_n):
                    remote(
                        results.at[j, packet(0)], relay_in.at[slot, j, packet(m)],
                        rb_send.at[near_n, j], rb_recv.at[slot, m, j], sp_peer(m),
                    ).wait_recv()
                relay_sum[slot, j] = weighed(1 + slot, relay_in[slot, j]).astype(jnp.bfloat16)
                summed_up(slot, j).start()

    band_results(0)
    direct(0)
    band_results(1)
    relay_band(0)
    band_results(2)
    relay_band(1)
    band_results(3)
    for j in range(1, blocks):
        direct(j)
    relay_band(2)
    relay_band(3)

    def finish(j):
        cols = slice(j * band, (j + 1) * band)
        for mask in range(1, near_n):
            give_back[mask, j].wait_recv()
        remote(
            relay_sum.at[0, j], far_in.at[j], sum_send.at[0, j], sum_recv.at[j], (relay, me_t)
        ).wait_recv()
        total = stream[:, cols] + weighed(0, returned[j]) + far_in[j].astype(jnp.float32)
        out_ref[:, cols] = total.astype(jnp.bfloat16)

    finish(0)
    finish(1)
    finish(2)
    finish(3)

    own_copies = rim_copies + route_copies + list(across) + list(forward) + beside + far_rows
    for copy in own_copies + list(exchange.values()) + list(dispatch.values()) + list(give_back.values()):
        copy.wait_send()

    @pl.when(in_middle)
    def _():
        for slot in range(2):
            for h in range(halves):
                for m in range(1, near_n):
                    relayed(slot, m, h).wait_send()
            for j in range(blocks):
                summed_up(slot, j).wait_send()
        for j in range(blocks):
            for mask, m, slot in from_middle:
                to_relay(mask, m, slot, j).wait_send()

    @pl.when(at_end)
    def _():
        for j in range(blocks):
            for mask, m, slot in from_end:
                to_relay(mask, m, slot, j).wait_send()


def shards(*args):
    (residual, conv_value, conv_gate, segments, conv_weight, norm_gain, norm_shift, out_weight,
     ffn_gain, routes, route_weights, w_gate, w_up, w_down) = args
    tok_dev, local = conv_value.shape
    width = residual.shape[1]
    experts_n, columns = lax.axis_size("sp"), lax.axis_size("tp")
    top_count = routes.shape[1]
    capacity = max(2, 2 * tok_dev * top_count // (columns * experts_n))
    if capacity % 32 or columns != 4 or tok_dev != columns * 128 or experts_n != 8:
        return plain_shards(*args)
    rows_own = tok_dev // columns
    lanes = DC // CONV_GROUPS
    slot_total = experts_n * capacity
    near_slots = slot_total // 2
    halves, blocks = 2, 4
    half, band = width // halves, width // blocks
    bf16, f32 = jnp.bfloat16, jnp.float32
    vmem, dma = pltpu.VMEM, pltpu.SemaphoreType.DMA
    spec, anywhere = pl.BlockSpec(memory_space=pltpu.VMEM), pl.BlockSpec(memory_space=pl.ANY)
    specs = [spec] * 14
    for i in (0, 1, 2, 7, 11, 12, 13):
        specs[i] = anywhere
    routes_t, route_weights_t = routes.T, route_weights.T
    return pl.pallas_call(
        functools.partial(layer_kernel, experts_n, columns, capacity, blocks),
        out_shape=jax.ShapeDtypeStruct((rows_own, width), bf16),
        in_specs=specs,
        out_specs=spec,
        scratch_shapes=[
            vmem((rows_own, width), bf16), vmem((tok_dev, local), bf16), vmem((tok_dev, local), bf16),
            vmem(out_weight.shape, bf16),
            vmem((width, local), bf16), vmem((width, local), bf16), vmem((local, width), bf16),
            vmem((3, width, local), bf16), vmem((3, width, local), bf16), vmem((3, local, width), bf16),
            vmem((2, RIM, local), bf16), vmem((tok_dev // lanes, lanes), jnp.int32),
            vmem((RIM + tok_dev, lanes), f32), vmem((RIM + tok_dev, local), f32),
            vmem((RIM + 64, local), f32), vmem((RIM + 64, lanes), f32),
            vmem((tok_dev, local), bf16), vmem((columns, rows_own, local), bf16),
            vmem((rows_own, width), f32), vmem((halves, rows_own, half), bf16),
            vmem((halves, near_slots, half), bf16), vmem((halves, slot_total, half), bf16),
            vmem((2, halves, rows_own, half), bf16), vmem((2, halves, near_slots, half), bf16),
            vmem((columns, slot_total, local), bf16), vmem((slot_total, band), f32),
            vmem((blocks, slot_total, band), bf16), vmem((blocks, near_slots, band), bf16),
            vmem((2, blocks, near_slots, band), bf16), vmem((2, blocks, rows_own, band), bf16),
            vmem((blocks, rows_own, band), bf16),
            vmem((3, top_count, rows_own, near_slots), bf16), vmem((3, near_slots, rows_own), bf16),
            vmem((3, top_count, rows_own, rows_own), f32),
            vmem((2, *routes_t.shape), routes.dtype), vmem((2, *route_weights_t.shape), route_weights.dtype),
            dma((7,)), dma((4 + blocks,)), dma((4 + blocks,)), dma((3,)), dma((3,)),
            dma((4 + blocks,)), dma((4 + blocks,)), dma((3,)), dma((3,)), dma((columns,)), dma((columns,)),
            dma((2,)), dma((2, 2)), dma((halves,)), dma((2, halves)),
            dma((experts_n // 2, halves)), dma((experts_n, halves)), dma((2, experts_n // 2, halves)),
            dma((experts_n, blocks)), dma((2, experts_n // 2, blocks)),
            dma((experts_n // 2, blocks)), dma((experts_n // 2, blocks)), dma((2, blocks)), dma((blocks,)),
        ],
        compiler_params=pltpu.CompilerParams(
            collective_id=0, has_side_effects=True, vmem_limit_bytes=60 * 1024 * 1024
        ),
    )(
        residual, conv_value, conv_gate,
        segments.reshape(-1, lanes), conv_weight,
        norm_gain[None], norm_shift[None], out_weight, ffn_gain[None],
        routes_t, route_weights_t, w_gate[0], w_up[0], w_down[0],
    )


def solution(mesh):
    return jax.shard_map(
        shards,
        mesh=mesh,
        in_specs=(
            P(("sp", "tp"), None),
            P("sp", "tp"),
            P("sp", "tp"),
            P("sp"),
            P(None, "tp"),
            P("tp"),
            P("tp"),
            P(),
            P(),
            P("sp", None),
            P("sp", None),
            P("sp", None, "tp"),
            P("sp", None, "tp"),
            P("sp", "tp", None),
        ),
        out_specs=P(("sp", "tp"), None),
        check_vma=False,
    )
```

time: 136 us -> 108 us (0.79)
  Pallas kernels: 134 us -> 106 us
    pallas_call x1, Pallas kernels: 134 us -> 106 us  [shards(): pl.pallas_call(functools.partial(layer_kernel, experts_n, columns, capaci...]
where the time goes in v1:
time: 108 us; the launch traced here: 107 us
  Pallas kernels  106 us (98%)
  local copies, waits for them, and re-layouts  1.88 us (2%)
    pallas_call x1, Pallas kernels, shards(): pl.pallas_call(functools.partial(layer_kernel, experts_n, columns, capaci...  106 us

profile of v1, /device:TPU:0, one launch (start us, length us, event | category | flops | bytes accessed | tf_op | source)
XLA Modules:
  0.0 107.4 jit_solution(3017754674132203110)
XLA Ops:
  0.0 105.5 %shard_map.136 = bf16[128,2048]{1,0:T(8,128)(2,1)} custom-call(bf16[128,2048]{1,0:T(8,128)(2,1)} %residual_hbm.1, bf16[512,256]{1,0:T(8,128)(2,1)} %value_hbm.1, bf16[512,256]{1,0:T(8,128)(2,1)} %gate_hbm.1, s32[4,128]{1,0:T(4,128)} %bitcast.15, f32[31,256]{1,0:T(8,128)} %conv_w_ref.1, f32[1,256]{1,0:T(1,128)} %bitcast.16, f32[1,256]{1,0:T(1,128)} %bitcast.17, ...), custom_call_target="tpu_custom_call" | custom-call | tf_op jit(solution)/shard_map/pallas_call | solution.py:624
  105.5 1.9 %copy.16 = bf16[128,2048]{1,0:T(8,128)(2,1)} copy(bf16[128,2048]{1,0:T(8,128)(2,1)} %shard_map.136) | data formatting | bytes 1048576

commit v2 on v1

--- a/solution.py
+++ b/solution.py
@@ -130,15 +130,16 @@
 
 def layer_kernel(
     experts_n, columns, capacity, blocks,
-    residual_hbm, value_hbm, gate_hbm, seg_ref, conv_w_ref, gain_ref, shift_ref, ow_hbm, ffn_ref,
-    routes_ref, route_w_ref, wg_hbm, wu_hbm, wd_hbm,
-    out_ref,
-    residual, value, gate, ow, wg, wu, wd, wg_in, wu_in, wd_in, rim, seg_in, seg_ext, ext, win, seg_win,
-    conv_out, conv_in, stream, normed, outgoing, arrived, rows_in, relay_out, hidden, partial,
+    residual_hbm, value_hbm, gate_hbm, seg_hbm, conv_w_hbm, gain_hbm, shift_hbm, ow_hbm, ffn_hbm,
+    routes_hbm, route_w_hbm, wg_hbm, wu_hbm, wd_hbm,
+    out_hbm,
+    residual, value, gate, seg_ref, conv_w_ref, gain_ref, shift_ref, ow, ffn_ref, routes_ref, route_w_ref,
+    wg, wu, wd, out_ref, wg_in, wu_in, wd_in, rim, seg_in, seg_ext, ext, win, seg_win,
+    conv_out, conv_in, stream, normed, outgoing, arrived, rows_in, relay_out, hidden, silu_gate, partial,
     results, returned, relay_in, relay_sum, far_in, tables, picks, shares, routes_in, route_w_in,
     load_sem, y_send, y_recv, c_send, c_recv, f_send, f_recv, rim_send, rim_recv, x_send, x_recv,
-    t_send, t_recv, far_send, far_recv, d_send, d_recv, rd_send,
-    rb_send, rb_recv, r_send, r_recv, sum_send, sum_recv,
+    t_send, t_recv, far_send, far_recv, d_send, d_recv, e_recv, rd_send,
+    rb_send, rb_recv, r_send, r_recv, sum_send, sum_recv, out_sem,
 ):
     me_s, me_t = lax.axis_index("sp"), lax.axis_index("tp")
     tok_dev, local = value.shape
@@ -167,10 +168,13 @@
     loads = [
         pltpu.make_async_copy(src, dst, load_sem.at[i])
         for i, (src, dst) in enumerate((
-            (value_hbm, value), (gate_hbm, gate), (residual_hbm, residual), (ow_hbm, ow),
+            (value_hbm, value), (gate_hbm, gate), (seg_hbm, seg_ref), (conv_w_hbm, conv_w_ref),
+            (gain_hbm, gain_ref), (shift_hbm, shift_ref), (routes_hbm, routes_ref), (route_w_hbm, route_w_ref),
+            (residual_hbm, residual), (ow_hbm, ow), (ffn_hbm, ffn_ref),
             (wg_hbm, wg), (wu_hbm, wu), (wd_hbm, wd),
         ))
     ]
+    conv_loads, stream_loads = 8, 11
     barrier = pltpu.get_barrier_semaphore()
     peers = [tp_peer(mask) for mask in range(1, columns)]
     peers += [sp_peer(mask) for mask in range(1, experts_n)]
@@ -178,6 +182,8 @@
         pl.semaphore_signal(barrier, inc=1, device_id=peer, device_id_type=MESH)
     for load in loads:
         load.start()
+    for load in loads[:conv_loads]:
+        load.wait()
     pl.semaphore_wait(barrier, len(peers))
 
     def remote(src, dst, send, recv, peer):
@@ -190,7 +196,7 @@
     rim_copies = [
         remote(ref, dst, rim_send.at[i], rim_recv.at[i], (next_s, me_t))
         for i, (ref, dst) in enumerate(
-            ((value_hbm.at[last], rim.at[0]), (gate_hbm.at[last], rim.at[1]), (seg_ref, seg_in))
+            ((value.at[last], rim.at[0]), (gate.at[last], rim.at[1]), (seg_ref, seg_in))
         )
     ]
     for copy in rim_copies:
@@ -198,8 +204,8 @@
 
     def across_piece(i, own, into, rows, cols):
         return (
-            remote(own.at[rows, cols], into.at[1, rows, cols], y_send.at[i], y_recv.at[i], tp_peer(2)),
-            remote(into.at[1, rows, cols], into.at[2, rows, cols], f_send.at[i], f_recv.at[i], tp_peer(1)),
+            remote(own.at[rows, cols], into.at[1, rows, cols], y_send, y_recv.at[i], tp_peer(2)),
+            remote(into.at[1, rows, cols], into.at[2, rows, cols], f_send, f_recv.at[i], tp_peer(1)),
         )
 
     every, first_rows = pl.ds(0, local), width // 4
@@ -207,13 +213,14 @@
         (wg_hbm, wg_in, pl.ds(0, first_rows), every),
         (wg_hbm, wg_in, pl.ds(first_rows, width - first_rows), every),
         (wu_hbm, wu_in, pl.ds(0, width // 2), every),
-        (wu_hbm, wu_in, pl.ds(width // 2, width // 2), every),
+        (wu_hbm, wu_in, pl.ds(width // 2, width // 4), every),
+        (wu_hbm, wu_in, pl.ds(3 * width // 4, width // 4), every),
     ]
     up_done = len(pieces)
     pieces += [(wd_hbm, wd_in, every, pl.ds(j * band, band)) for j in range(blocks)]
     across, forward = zip(*[across_piece(i, *piece) for i, piece in enumerate(pieces)])
     beside = [
-        remote(own, into.at[0], c_send.at[i], c_recv.at[i], tp_peer(1))
+        remote(own, into.at[0], c_send, c_recv.at[i], tp_peer(1))
         for i, (own, into) in enumerate(((wg_hbm, wg_in), (wu_hbm, wu_in), (wd_hbm, wd_in)))
     ]
     across[0].start()
@@ -237,8 +244,6 @@
         ext[pl.ds(row + RIM, 64), :] = gated_of(value[pl.ds(row, 64), :], gate[pl.ds(row, 64), :])
         return carry
 
-    for load in loads[:2]:
-        load.wait()
     lax.fori_loop(0, tok_dev // 64, gate_rows, 0)
     lanes_n = seg_ref.shape[1]
 
@@ -248,58 +253,48 @@
     for i in range(seg_ref.shape[0]):
         seg_ext[RIM + i * lanes_n : RIM + (i + 1) * lanes_n, :] = column(seg_ref[i : i + 1, :])
 
-    for copy in rim_copies:
-        copy.wait_recv()
-    ext[pl.ds(0, RIM), :] = gated_of(rim[0], rim[1])
-    before = column(seg_in[seg_ref.shape[0] - 1 : seg_ref.shape[0], :])[lanes_n - RIM :, :]
-    seg_ext[0:RIM, :] = jnp.where(me_s == 0, -1.0, before)
-
     block = 64
     lead = RIM - (taps - 1)
 
     def conv_rows(row):
-        win[...] = ext[pl.ds(row, RIM + block), :]
-        seg_win[...] = seg_ext[pl.ds(row, RIM + block), :]
-        own_seg = seg_win[RIM:, :]
-        sums = [jnp.zeros((block, group), jnp.float32) for _ in range(local // group)]
-        for tap in range(taps):
-            at = lead + tap
-            same_doc = seg_win[at : at + block, :] == own_seg
+        win[...] = ext[pl.ds(row, RIM + rows_own), :]
+        seg_win[...] = seg_ext[pl.ds(row, RIM + rows_own), :]
+        for start in range(0, rows_own, block):
+            own_seg = seg_win[start + RIM : start + RIM + block, :]
+            sums = [jnp.zeros((block, group), jnp.float32) for _ in range(local // group)]
+            for tap in range(taps):
+                at = start + lead + tap
+                same_doc = seg_win[at : at + block, :] == own_seg
+                for g in range(local // group):
+                    lanes = slice(g * group, (g + 1) * group)
+                    term = win[at : at + block, lanes] * conv_w_ref[tap : tap + 1, lanes]
+                    sums[g] = sums[g] + jnp.where(same_doc, term, 0.0)
             for g in range(local // group):
                 lanes = slice(g * group, (g + 1) * group)
-                term = win[at : at + block, lanes] * conv_w_ref[tap : tap + 1, lanes]
-                sums[g] = sums[g] + jnp.where(same_doc, term, 0.0)
-        for g in range(local // group):
-            lanes = slice(g * group, (g + 1) * group)
-            mean = jnp.mean(sums[g], axis=-1, keepdims=True)
-            centred = sums[g] - mean
-            deviation = jnp.mean(centred * centred, axis=-1, keepdims=True)
-            scaled = centred * lax.rsqrt(deviation + 1e-05) * gain_ref[:, lanes] + shift_ref[:, lanes]
-            conv_out[pl.ds(row, block), lanes] = (scaled / (1.0 + jnp.exp(-scaled))).astype(jnp.bfloat16)
-
-    exchange = {}
-    for mask in (3, 2, 1, 0):
-        peer_row = pl.multiple_of(flipped(me_t, mask) * rows_own, rows_own)
-
-        def conv_step(i, carry):
-            conv_rows(pl.multiple_of(peer_row + i * block, block))
-            return carry
-
-        lax.fori_loop(0, rows_own // block, conv_step, 0)
-        if mask:
-            exchange[mask] = remote(
-                conv_out.at[pl.ds(peer_row, rows_own)], conv_in.at[mask],
-                x_send.at[mask], x_recv.at[mask], tp_peer(mask),
-            )
-            exchange[mask].start()
-        else:
+                mean = jnp.mean(sums[g], axis=-1, keepdims=True)
+                centred = sums[g] - mean
+                deviation = jnp.mean(centred * centred, axis=-1, keepdims=True)
+                scaled = centred * lax.rsqrt(deviation + 1e-05) * gain_ref[:, lanes] + shift_ref[:, lanes]
+                conv_out[pl.ds(row + start, block), lanes] = (scaled / (1.0 + jnp.exp(-scaled))).astype(jnp.bfloat16)
+
+    low = me_t % 2
+    masks = (3 - low, 2 + low, 1, 0)
+
+    def conv_part(i):
+        peer_row = pl.multiple_of((me_t ^ masks[i]) * rows_own, rows_own)
+        conv_rows(peer_row)
+        if i == 3:
             conv_in[0] = conv_out[pl.ds(peer_row, rows_own), :]
-        if mask == 2:
-            for copy in across[1:]:
-                copy.start()
-
-    for copy in beside:
+            return []
+        copy = remote(
+            conv_out.at[pl.ds(peer_row, rows_own)], conv_in.at[masks[i]], x_send, x_recv,
+            (me_s, me_t ^ masks[i]),
+        )
         copy.start()
+        return [copy]
+
+    conv_part(0)
+
     numbers = lax.broadcasted_iota(jnp.int32, (rows_own, lanes_n), 1).astype(jnp.float32)
     earlier = jnp.where(
         lax.broadcasted_iota(jnp.int32, (rows_own, rows_own), 0)
@@ -327,6 +322,20 @@
         0, lambda m: routes_ref[m : m + 1, own_lanes], lambda m: route_w_ref[m : m + 1, own_lanes]
     )
 
+    for copy in rim_copies:
+        copy.wait_recv()
+    ext[pl.ds(0, RIM), :] = gated_of(rim[0], rim[1])
+    before = column(seg_in[seg_ref.shape[0] - 1 : seg_ref.shape[0], :])[lanes_n - RIM :, :]
+    seg_ext[0:RIM, :] = jnp.where(me_s == 0, -1.0, before)
+
+    conv_part(1)
+    for copy in across[1:]:
+        copy.start()
+    conv_part(2)
+    for copy in beside:
+        copy.start()
+    conv_part(3)
+
     @pl.when(in_middle)
     def _():
         for slot in range(2):
@@ -341,10 +350,10 @@
 
     across[0].wait_recv()
     forward[0].start()
-    for load in loads[2:4]:
+    for load in loads[conv_loads:stream_loads]:
         load.wait()
-    for mask in (1, 2, 3):
-        exchange[mask].wait_recv()
+    swapped = remote(conv_in.at[pl.ds(1, columns - 1)], conv_in.at[pl.ds(1, columns - 1)], x_send, x_recv, tp_peer(1))
+    swapped.wait_recv()
 
     squares = jnp.zeros((rows_own, 1), jnp.float32)
     for col in range(0, width, tile):
@@ -369,7 +378,7 @@
     def packet(mask):
         return pl.ds(mask * capacity, capacity)
 
-    dispatch = {}
+    others = pl.ds(capacity, near_slots - capacity)
     for h in range(halves):
         for col in range(0, half, tile):
             cols = slice(col, col + tile)
@@ -377,11 +386,9 @@
                 picks[0], normed[h, :, cols], preferred_element_type=jnp.float32
             ).astype(jnp.bfloat16)
         for mask in range(near_n - 1, 0, -1):
-            dispatch[mask, h] = remote(
-                outgoing.at[h, packet(mask)], arrived.at[h, packet(mask)],
-                d_send.at[mask, h], d_recv.at[mask, h], sp_peer(mask),
-            )
-            dispatch[mask, h].start()
+            remote(
+                outgoing.at[h, packet(mask)], arrived.at[h, packet(mask)], d_send, d_recv, sp_peer(mask)
+            ).start()
         arrived[h, 0:capacity, :] = outgoing[h, 0:capacity, :]
 
     relay_masks = ((6, 7, 4, 5), (4, 5, 6, 7))
@@ -389,63 +396,58 @@
     def relayed(slot, m, h):
         return remote(
             relay_out.at[slot, h, packet(m)], arrived.at[h, packet(relay_masks[slot][m])],
-            rd_send.at[slot, m, h], d_recv.at[relay_masks[slot][m], h], sp_peer(m),
-        )
-
-    def relay_half(h):
+            rd_send, e_recv, sp_peer(m),
+        )
+
+    def relay_half(slot, h):
         @pl.when(in_middle)
         def _():
-            for slot in range(2):
-                remote(
-                    normed.at[h], rows_in.at[slot, h], far_send.at[h], far_recv.at[slot, h], (relay, me_t)
-                ).wait_recv()
-                for col in range(0, half, tile):
-                    cols = slice(col, col + tile)
-                    relay_out[slot, h, :, cols] = jnp.dot(
-                        picks[1 + slot], rows_in[slot, h, :, cols], preferred_element_type=jnp.float32
-                    ).astype(jnp.bfloat16)
-                for m in (2, 3, 1):
-                    relayed(slot, m, h).start()
-                place = relay_masks[slot][0] * capacity
-                arrived[h, place : place + capacity, :] = relay_out[slot, h, 0:capacity, :]
-
-    def d_wait(mask, h):
-        remote(
-            outgoing.at[h, packet(0)], arrived.at[h, packet(mask)],
-            d_send.at[0, h], d_recv.at[mask, h], sp_peer(1),
-        ).wait_recv()
-
-    relay_half(0)
-
-    for load in loads[4:]:
+            remote(
+                normed.at[h], rows_in.at[slot, h], far_send.at[h], far_recv.at[slot, h], (relay, me_t)
+            ).wait_recv()
+            for col in range(0, half, tile):
+                cols = slice(col, col + tile)
+                relay_out[slot, h, :, cols] = jnp.dot(
+                    picks[1 + slot], rows_in[slot, h, :, cols], preferred_element_type=jnp.float32
+                ).astype(jnp.bfloat16)
+            for m in (2, 3, 1):
+                relayed(slot, m, h).start()
+            place = relay_masks[slot][0] * capacity
+            arrived[h, place : place + capacity, :] = relay_out[slot, h, 0:capacity, :]
+
+    def landed(rows, recv):
+        remote(arrived.at[:, rows], arrived.at[:, rows], d_send, recv, sp_peer(1)).wait_recv()
+
+    for h in range(halves):
+        relay_half(1, h)
+
+    for load in loads[stream_loads:]:
         load.wait()
     for copy in beside:
         copy.wait_recv()
     across[1].wait_recv()
     forward[1].start()
 
-    for h in range(1, halves):
-        relay_half(h)
-
     for h in range(halves):
-        for mask in range(1, near_n):
-            d_wait(mask, h)
+        relay_half(0, h)
+
+    landed(others, d_recv)
 
     near, far = slice(0, near_slots), slice(near_slots, 2 * near_slots)
-    whole = slice(0, 2 * near_slots)
+
+    def act(w, rows):
+        return sum(
+            jnp.dot(arrived[h, rows, :], w[h * half : (h + 1) * half, :], preferred_element_type=jnp.float32)
+            for h in range(halves)
+        )
+
+    def silu(v):
+        return v / (1.0 + jnp.exp(-v))
 
     def hidden_units(mask, rows):
         g = wg if mask == 0 else wg_in.at[mask - 1]
         u = wu if mask == 0 else wu_in.at[mask - 1]
-
-        def act(w):
-            return sum(
-                jnp.dot(arrived[h, rows, :], w[h * half : (h + 1) * half, :], preferred_element_type=jnp.float32)
-                for h in range(halves)
-            )
-
-        gate_act, up_act = act(g), act(u)
-        hidden[mask, rows, :] = (gate_act / (1.0 + jnp.exp(-gate_act)) * up_act).astype(jnp.bfloat16)
+        hidden[mask, rows, :] = (silu(act(g, rows)) * act(u, rows)).astype(jnp.bfloat16)
 
     hidden_units(0, near)
     hidden_units(1, near)
@@ -453,15 +455,13 @@
     across[2].wait_recv()
     forward[2].start()
 
-    for h in range(halves):
-        for mask in range(near_n + 1, experts_n, 2):
-            d_wait(mask, h)
+    @pl.when(in_middle)
+    def _():
+        landed(pl.ds(near_slots, 2 * capacity), e_recv)
 
     @pl.when(at_end)
     def _():
-        for h in range(halves):
-            for mask in range(near_n, experts_n, 2):
-                d_wait(mask, h)
+        landed(pl.ds(near_slots, 4 * capacity), e_recv)
 
     hidden_units(0, far)
     hidden_units(1, far)
@@ -469,17 +469,31 @@
     across[3].wait_recv()
     forward[3].start()
 
-    hidden_units(2, whole)
-
-    for i in range(up_done):
+    for i in range(2):
         forward[i].wait_recv()
-
-    hidden_units(3, whole)
+    for mask in (2, 3):
+        for rows in (near, far):
+            silu_gate[mask - 2, rows, :] = silu(act(wg_in.at[mask - 1], rows))
+
+    across[4].wait_recv()
+    forward[4].start()
+
+    def finish_hidden(mask):
+        for rows in (near, far):
+            units = silu_gate[mask - 2, rows, :] * act(wu_in.at[mask - 1], rows)
+            hidden[mask, rows, :] = units.astype(jnp.bfloat16)
+
+    finish_hidden(2)
+
+    for i in range(2, up_done):
+        forward[i].wait_recv()
+
+    finish_hidden(3)
 
     def to_relay(mask, m, slot, j):
         return remote(
             results.at[j, packet(mask)], relay_in.at[slot, j, packet(m)],
-            rb_send.at[mask, j], rb_recv.at[slot, m, j], sp_peer(m),
+            rb_send, rb_recv.at[slot, j], sp_peer(m),
         )
 
     from_middle = ((7, 1, 0), (5, 1, 1))
@@ -488,7 +502,7 @@
     give_back = {
         (mask, j): remote(
             results.at[j, packet(mask)], returned.at[j, packet(mask)],
-            r_send.at[mask, j], r_recv.at[mask, j], sp_peer(mask),
+            r_send, r_recv.at[j], sp_peer(mask),
         )
         for j in range(blocks) for mask in range(1, near_n)
     }
@@ -526,7 +540,7 @@
 
     def summed_up(slot, j):
         return remote(
-            relay_sum.at[slot, j], far_in.at[j], sum_send.at[slot, j], sum_recv.at[j],
+            relay_sum.at[slot, j], far_in.at[j], sum_send, sum_recv.at[j],
             sp_peer((6, 4)[slot]),
         )
 
@@ -540,62 +554,74 @@
         @pl.when(in_middle)
         def _():
             for slot in range(2):
-                for m in range(1, near_n):
-                    remote(
-                        results.at[j, packet(0)], relay_in.at[slot, j, packet(m)],
-                        rb_send.at[near_n, j], rb_recv.at[slot, m, j], sp_peer(m),
-                    ).wait_recv()
+                remote(
+                    relay_in.at[slot, j, others], relay_in.at[slot, j, others],
+                    rb_send, rb_recv.at[slot, j], sp_peer(1),
+                ).wait_recv()
                 relay_sum[slot, j] = weighed(1 + slot, relay_in[slot, j]).astype(jnp.bfloat16)
                 summed_up(slot, j).start()
 
-    band_results(0)
-    direct(0)
-    band_results(1)
-    relay_band(0)
-    band_results(2)
-    relay_band(1)
-    band_results(3)
-    for j in range(1, blocks):
-        direct(j)
-    relay_band(2)
-    relay_band(3)
+    early, lag = blocks // 4, blocks // 2
+    for j in range(blocks):
+        band_results(j)
+        if j < early:
+            direct(j)
+        else:
+            pl.when(in_middle)(functools.partial(direct, j))
+        if j >= lag:
+            relay_band(j - lag)
+    for j in range(early, blocks):
+        pl.when(at_end)(functools.partial(direct, j))
+    for j in range(blocks - lag, blocks):
+        relay_band(j)
+
+    outs = [
+        pltpu.make_async_copy(
+            out_ref.at[:, pl.ds(j * band, band)], out_hbm.at[:, pl.ds(j * band, band)], out_sem.at[j]
+        )
+        for j in range(blocks)
+    ]
 
     def finish(j):
         cols = slice(j * band, (j + 1) * band)
-        for mask in range(1, near_n):
-            give_back[mask, j].wait_recv()
         remote(
-            relay_sum.at[0, j], far_in.at[j], sum_send.at[0, j], sum_recv.at[j], (relay, me_t)
+            relay_sum.at[0, j], far_in.at[j], sum_send, sum_recv.at[j], (relay, me_t)
+        ).wait_recv()
+        remote(
+            returned.at[j, others], returned.at[j, others], r_send, r_recv.at[j], sp_peer(1)
         ).wait_recv()
         total = stream[:, cols] + weighed(0, returned[j]) + far_in[j].astype(jnp.float32)
         out_ref[:, cols] = total.astype(jnp.bfloat16)
-
-    finish(0)
-    finish(1)
-    finish(2)
-    finish(3)
-
-    own_copies = rim_copies + route_copies + list(across) + list(forward) + beside + far_rows
-    for copy in own_copies + list(exchange.values()) + list(dispatch.values()) + list(give_back.values()):
+        outs[j].start()
+
+    for j in range(blocks // 2):
+        finish(j)
+    for j in range(blocks // 2, blocks):
+        finish(j)
+
+    def sent(ref, sem):
+        remote(ref, ref, sem, sem, sp_peer(1)).wait_send()
+
+    for copy in rim_copies + route_copies + far_rows:
         copy.wait_send()
+    for sem in (y_send, f_send, c_send):
+        sent(wg_in, sem)
+    swapped.wait_send()
+    sent(outgoing.at[:, others], d_send)
+    sent(results.at[:, others], r_send)
 
     @pl.when(in_middle)
     def _():
-        for slot in range(2):
-            for h in range(halves):
-                for m in range(1, near_n):
-                    relayed(slot, m, h).wait_send()
-            for j in range(blocks):
-                summed_up(slot, j).wait_send()
-        for j in range(blocks):
-            for mask, m, slot in from_middle:
-                to_relay(mask, m, slot, j).wait_send()
+        sent(relay_out.at[:, :, others], rd_send)
+        sent(relay_sum, sum_send)
+        sent(results.at[:, pl.ds(0, 2 * capacity)], rb_send)
 
     @pl.when(at_end)
     def _():
-        for j in range(blocks):
-            for mask, m, slot in from_end:
-                to_relay(mask, m, slot, j).wait_send()
+        sent(results.at[:, pl.ds(0, 4 * capacity)], rb_send)
+
+    for copy in outs:
+        copy.wait()
 
 
 def shards(*args):
@@ -612,55 +638,50 @@
     lanes = DC // CONV_GROUPS
     slot_total = experts_n * capacity
     near_slots = slot_total // 2
-    halves, blocks = 2, 4
+    halves, blocks = 2, 8
     half, band = width // halves, width // blocks
     bf16, f32 = jnp.bfloat16, jnp.float32
     vmem, dma = pltpu.VMEM, pltpu.SemaphoreType.DMA
-    spec, anywhere = pl.BlockSpec(memory_space=pltpu.VMEM), pl.BlockSpec(memory_space=pl.ANY)
-    specs = [spec] * 14
-    for i in (0, 1, 2, 7, 11, 12, 13):
-        specs[i] = anywhere
-    routes_t, route_weights_t = routes.T, route_weights.T
+    anywhere = pl.BlockSpec(memory_space=pl.ANY)
+    operands = (
+        residual, conv_value, conv_gate,
+        segments.reshape(-1, lanes), conv_weight,
+        norm_gain[None], norm_shift[None], out_weight, ffn_gain[None],
+        routes.T, route_weights.T, w_gate[0], w_up[0], w_down[0],
+    )
     return pl.pallas_call(
         functools.partial(layer_kernel, experts_n, columns, capacity, blocks),
         out_shape=jax.ShapeDtypeStruct((rows_own, width), bf16),
-        in_specs=specs,
-        out_specs=spec,
-        scratch_shapes=[
-            vmem((rows_own, width), bf16), vmem((tok_dev, local), bf16), vmem((tok_dev, local), bf16),
-            vmem(out_weight.shape, bf16),
-            vmem((width, local), bf16), vmem((width, local), bf16), vmem((local, width), bf16),
+        in_specs=[anywhere] * len(operands),
+        out_specs=anywhere,
+        scratch_shapes=[vmem(operand.shape, operand.dtype) for operand in operands] + [
+            vmem((rows_own, width), bf16),
             vmem((3, width, local), bf16), vmem((3, width, local), bf16), vmem((3, local, width), bf16),
             vmem((2, RIM, local), bf16), vmem((tok_dev // lanes, lanes), jnp.int32),
             vmem((RIM + tok_dev, lanes), f32), vmem((RIM + tok_dev, local), f32),
-            vmem((RIM + 64, local), f32), vmem((RIM + 64, lanes), f32),
+            vmem((RIM + rows_own, local), f32), vmem((RIM + rows_own, lanes), f32),
             vmem((tok_dev, local), bf16), vmem((columns, rows_own, local), bf16),
             vmem((rows_own, width), f32), vmem((halves, rows_own, half), bf16),
             vmem((halves, near_slots, half), bf16), vmem((halves, slot_total, half), bf16),
             vmem((2, halves, rows_own, half), bf16), vmem((2, halves, near_slots, half), bf16),
-            vmem((columns, slot_total, local), bf16), vmem((slot_total, band), f32),
+            vmem((columns, slot_total, local), bf16), vmem((2, slot_total, local), f32),
+            vmem((slot_total, band), f32),
             vmem((blocks, slot_total, band), bf16), vmem((blocks, near_slots, band), bf16),
             vmem((2, blocks, near_slots, band), bf16), vmem((2, blocks, rows_own, band), bf16),
             vmem((blocks, rows_own, band), bf16),
             vmem((3, top_count, rows_own, near_slots), bf16), vmem((3, near_slots, rows_own), bf16),
             vmem((3, top_count, rows_own, rows_own), f32),
-            vmem((2, *routes_t.shape), routes.dtype), vmem((2, *route_weights_t.shape), route_weights.dtype),
-            dma((7,)), dma((4 + blocks,)), dma((4 + blocks,)), dma((3,)), dma((3,)),
-            dma((4 + blocks,)), dma((4 + blocks,)), dma((3,)), dma((3,)), dma((columns,)), dma((columns,)),
+            vmem((2, top_count, tok_dev), routes.dtype), vmem((2, top_count, tok_dev), route_weights.dtype),
+            dma((len(operands),)), dma, dma((5 + blocks,)), dma, dma((3,)),
+            dma, dma((5 + blocks,)), dma((3,)), dma((3,)), dma, dma,
             dma((2,)), dma((2, 2)), dma((halves,)), dma((2, halves)),
-            dma((experts_n // 2, halves)), dma((experts_n, halves)), dma((2, experts_n // 2, halves)),
-            dma((experts_n, blocks)), dma((2, experts_n // 2, blocks)),
-            dma((experts_n // 2, blocks)), dma((experts_n // 2, blocks)), dma((2, blocks)), dma((blocks,)),
+            dma, dma, dma, dma,
+            dma, dma((2, blocks)), dma, dma((blocks,)), dma, dma((blocks,)), dma((blocks,)),
         ],
         compiler_params=pltpu.CompilerParams(
             collective_id=0, has_side_effects=True, vmem_limit_bytes=60 * 1024 * 1024
         ),
-    )(
-        residual, conv_value, conv_gate,
-        segments.reshape(-1, lanes), conv_weight,
-        norm_gain[None], norm_shift[None], out_weight, ffn_gain[None],
-        routes_t, route_weights_t, w_gate[0], w_up[0], w_down[0],
-    )
+    )(*operands)
 
 
 def solution(mesh):

time: 108 us -> 101 us (0.935)
  Pallas kernels: 106 us -> 99.4 us
    pallas_call x1, Pallas kernels: 106 us -> 99.4 us  [shards(): pl.pallas_call(functools.partial(layer_kernel, experts_n, columns, capaci...]
where the time goes in v2:
time: 101 us
  Pallas kernels  99.4 us (98%)
  local copies, waits for them, and re-layouts  1.88 us (2%)
    pallas_call x1, Pallas kernels, shards(): pl.pallas_call(functools.partial(layer_kernel, experts_n, columns, capaci...  99.4 us

profile of v2, /device:TPU:0, one launch (start us, length us, event | category | flops | bytes accessed | tf_op | source)
XLA Modules:
  0.0 101.3 jit_solution(16853894439787929784)
XLA Ops:
  0.0 99.4 %shard_map.136 = bf16[128,2048]{1,0:T(8,128)(2,1)} custom-call(bf16[128,2048]{1,0:T(8,128)(2,1)} %residual_hbm.1, bf16[512,256]{1,0:T(8,128)(2,1)} %value_hbm.1, bf16[512,256]{1,0:T(8,128)(2,1)} %gate_hbm.1, s32[4,128]{1,0:T(4,128)} %bitcast.15, f32[31,256]{1,0:T(8,128)} %conv_w_hbm.1, f32[1,256]{1,0:T(1,128)} %bitcast.16, f32[1,256]{1,0:T(1,128)} %bitcast.17, ...), custom_call_target="tpu_custom_call" | custom-call | tf_op jit(solution)/shard_map/pallas_call | solution.py:652
  99.4 1.9 %copy.16 = bf16[128,2048]{1,0:T(8,128)(2,1)} copy(bf16[128,2048]{1,0:T(8,128)(2,1)} %shard_map.136) | data formatting | bytes 1048576

commit v3 on v2

--- a/solution.py
+++ b/solution.py
@@ -132,14 +132,14 @@
     experts_n, columns, capacity, blocks,
     residual_hbm, value_hbm, gate_hbm, seg_hbm, conv_w_hbm, gain_hbm, shift_hbm, ow_hbm, ffn_hbm,
     routes_hbm, route_w_hbm, wg_hbm, wu_hbm, wd_hbm,
-    out_hbm,
+    out_ref,
     residual, value, gate, seg_ref, conv_w_ref, gain_ref, shift_ref, ow, ffn_ref, routes_ref, route_w_ref,
-    wg, wu, wd, out_ref, wg_in, wu_in, wd_in, rim, seg_in, seg_ext, ext, win, seg_win,
+    wg, wu, wd, wg_in, wu_in, wd_in, rim, seg_in, seg_ext, ext, win, seg_win,
     conv_out, conv_in, stream, normed, outgoing, arrived, rows_in, relay_out, hidden, silu_gate, partial,
     results, returned, relay_in, relay_sum, far_in, tables, picks, shares, routes_in, route_w_in,
     load_sem, y_send, y_recv, c_send, c_recv, f_send, f_recv, rim_send, rim_recv, x_send, x_recv,
     t_send, t_recv, far_send, far_recv, d_send, d_recv, e_recv, rd_send,
-    rb_send, rb_recv, r_send, r_recv, sum_send, sum_recv, out_sem,
+    rb_send, rb_recv, r_send, r_recv, sum_send, sum_recv,
 ):
     me_s, me_t = lax.axis_index("sp"), lax.axis_index("tp")
     tok_dev, local = value.shape
@@ -208,10 +208,11 @@
             remote(into.at[1, rows, cols], into.at[2, rows, cols], f_send, f_recv.at[i], tp_peer(1)),
         )
 
-    every, first_rows = pl.ds(0, local), width // 4
+    every, first_rows, second_rows = pl.ds(0, local), width // 8, width // 16
     pieces = [
         (wg_hbm, wg_in, pl.ds(0, first_rows), every),
-        (wg_hbm, wg_in, pl.ds(first_rows, width - first_rows), every),
+        (wg_hbm, wg_in, pl.ds(first_rows, second_rows), every),
+        (wg_hbm, wg_in, pl.ds(first_rows + second_rows, width - first_rows - second_rows), every),
         (wu_hbm, wu_in, pl.ds(0, width // 2), every),
         (wu_hbm, wu_in, pl.ds(width // 2, width // 4), every),
         (wu_hbm, wu_in, pl.ds(3 * width // 4, width // 4), every),
@@ -294,6 +295,7 @@
         return [copy]
 
     conv_part(0)
+    across[1].start()
 
     numbers = lax.broadcasted_iota(jnp.int32, (rows_own, lanes_n), 1).astype(jnp.float32)
     earlier = jnp.where(
@@ -329,7 +331,7 @@
     seg_ext[0:RIM, :] = jnp.where(me_s == 0, -1.0, before)
 
     conv_part(1)
-    for copy in across[1:]:
+    for copy in across[2:]:
         copy.start()
     conv_part(2)
     for copy in beside:
@@ -348,8 +350,9 @@
                 lambda m: route_w_in[slot, m : m + 1, own_lanes],
             )
 
-    across[0].wait_recv()
-    forward[0].start()
+    for i in range(2):
+        across[i].wait_recv()
+        forward[i].start()
     for load in loads[conv_loads:stream_loads]:
         load.wait()
     swapped = remote(conv_in.at[pl.ds(1, columns - 1)], conv_in.at[pl.ds(1, columns - 1)], x_send, x_recv, tp_peer(1))
@@ -425,8 +428,8 @@
         load.wait()
     for copy in beside:
         copy.wait_recv()
-    across[1].wait_recv()
-    forward[1].start()
+    across[2].wait_recv()
+    forward[2].start()
 
     for h in range(halves):
         relay_half(0, h)
@@ -452,8 +455,8 @@
     hidden_units(0, near)
     hidden_units(1, near)
 
-    across[2].wait_recv()
-    forward[2].start()
+    across[3].wait_recv()
+    forward[3].start()
 
     @pl.when(in_middle)
     def _():
@@ -466,17 +469,17 @@
     hidden_units(0, far)
     hidden_units(1, far)
 
-    across[3].wait_recv()
-    forward[3].start()
-
-    for i in range(2):
+    across[4].wait_recv()
+    forward[4].start()
+
+    for i in range(3):
         forward[i].wait_recv()
     for mask in (2, 3):
         for rows in (near, far):
             silu_gate[mask - 2, rows, :] = silu(act(wg_in.at[mask - 1], rows))
 
-    across[4].wait_recv()
-    forward[4].start()
+    across[5].wait_recv()
+    forward[5].start()
 
     def finish_hidden(mask):
         for rows in (near, far):
@@ -485,7 +488,7 @@
 
     finish_hidden(2)
 
-    for i in range(2, up_done):
+    for i in range(3, up_done):
         forward[i].wait_recv()
 
     finish_hidden(3)
@@ -534,8 +537,8 @@
 
         returned[j, 0:capacity, :] = results[j, 0:capacity, :]
 
-    def direct(j):
-        for mask in range(near_n - 1, 0, -1):
+    def direct(j, masks):
+        for mask in masks:
             give_back[mask, j].start()
 
     def summed_up(slot, j):
@@ -564,23 +567,17 @@
     early, lag = blocks // 4, blocks // 2
     for j in range(blocks):
         band_results(j)
+        pl.when(in_middle)(functools.partial(direct, j, (3, 2)))
         if j < early:
-            direct(j)
-        else:
-            pl.when(in_middle)(functools.partial(direct, j))
+            pl.when(at_end)(functools.partial(direct, j, (3, 2)))
         if j >= lag:
             relay_band(j - lag)
-    for j in range(early, blocks):
-        pl.when(at_end)(functools.partial(direct, j))
+    for j in range(blocks):
+        if j >= early:
+            pl.when(at_end)(functools.partial(direct, j, (3, 2)))
+        direct(j, (1,))
     for j in range(blocks - lag, blocks):
         relay_band(j)
-
-    outs = [
-        pltpu.make_async_copy(
-            out_ref.at[:, pl.ds(j * band, band)], out_hbm.at[:, pl.ds(j * band, band)], out_sem.at[j]
-        )
-        for j in range(blocks)
-    ]
 
     def finish(j):
         cols = slice(j * band, (j + 1) * band)
@@ -592,7 +589,6 @@
         ).wait_recv()
         total = stream[:, cols] + weighed(0, returned[j]) + far_in[j].astype(jnp.float32)
         out_ref[:, cols] = total.astype(jnp.bfloat16)
-        outs[j].start()
 
     for j in range(blocks // 2):
         finish(j)
@@ -619,9 +615,6 @@
     @pl.when(at_end)
     def _():
         sent(results.at[:, pl.ds(0, 4 * capacity)], rb_send)
-
-    for copy in outs:
-        copy.wait()
 
 
 def shards(*args):
@@ -651,11 +644,10 @@
     )
     return pl.pallas_call(
         functools.partial(layer_kernel, experts_n, columns, capacity, blocks),
-        out_shape=jax.ShapeDtypeStruct((rows_own, width), bf16),
+        out_shape=pltpu.VMEM((rows_own, width), bf16),
         in_specs=[anywhere] * len(operands),
-        out_specs=anywhere,
+        out_specs=pl.BlockSpec(memory_space=pltpu.VMEM),
         scratch_shapes=[vmem(operand.shape, operand.dtype) for operand in operands] + [
-            vmem((rows_own, width), bf16),
             vmem((3, width, local), bf16), vmem((3, width, local), bf16), vmem((3, local, width), bf16),
             vmem((2, RIM, local), bf16), vmem((tok_dev // lanes, lanes), jnp.int32),
             vmem((RIM + tok_dev, lanes), f32), vmem((RIM + tok_dev, local), f32),
@@ -672,11 +664,11 @@
             vmem((3, top_count, rows_own, near_slots), bf16), vmem((3, near_slots, rows_own), bf16),
             vmem((3, top_count, rows_own, rows_own), f32),
             vmem((2, top_count, tok_dev), routes.dtype), vmem((2, top_count, tok_dev), route_weights.dtype),
-            dma((len(operands),)), dma, dma((5 + blocks,)), dma, dma((3,)),
-            dma, dma((5 + blocks,)), dma((3,)), dma((3,)), dma, dma,
+            dma((len(operands),)), dma, dma((6 + blocks,)), dma, dma((3,)),
+            dma, dma((6 + blocks,)), dma((3,)), dma((3,)), dma, dma,
             dma((2,)), dma((2, 2)), dma((halves,)), dma((2, halves)),
             dma, dma, dma, dma,
-            dma, dma((2, blocks)), dma, dma((blocks,)), dma, dma((blocks,)), dma((blocks,)),
+            dma, dma((2, blocks)), dma, dma((blocks,)), dma, dma((blocks,)),
         ],
         compiler_params=pltpu.CompilerParams(
             collective_id=0, has_side_effects=True, vmem_limit_bytes=60 * 1024 * 1024

time: 101 us -> 98.7 us (0.977)
  Pallas kernels: 99.4 us -> 97.8 us
  local copies, waits for them, and re-layouts: 1.88 us -> 0.8 us
    pallas_call x1, Pallas kernels: 99.4 us -> 97.8 us  [shards(): pl.pallas_call(functools.partial(layer_kernel, experts_n, columns, capaci...]
    unnamed x1, local copies, waits for them, and re-layouts: 1.88 us -> 0.8 us
where the time goes in v3:
time: 98.7 us; the launch traced here: 98.6 us
  Pallas kernels  97.8 us (99%)
    pallas_call x1, Pallas kernels, shards(): pl.pallas_call(functools.partial(layer_kernel, experts_n, columns, capaci...  97.8 us

profile of v3, /device:TPU:0, one launch (start us, length us, event | category | flops | bytes accessed | tf_op | source)
XLA Modules:
  0.0 98.6 jit_solution(3422851391033763880)
XLA Ops:
  0.0 97.8 %shard_map.136 = bf16[128,2048]{1,0:T(8,128)(2,1)S(1)} custom-call(bf16[128,2048]{1,0:T(8,128)(2,1)} %residual_hbm.1, bf16[512,256]{1,0:T(8,128)(2,1)} %value_hbm.1, bf16[512,256]{1,0:T(8,128)(2,1)} %gate_hbm.1, s32[4,128]{1,0:T(4,128)} %bitcast.15, f32[31,256]{1,0:T(8,128)} %conv_w_hbm.1, f32[1,256]{1,0:T(1,128)} %bitcast.16, f32[1,256]{1,0:T(1,128)} %bitcast.17, ...), custom_call_target="tpu_custom_call" | custom-call | tf_op jit(solution)/shard_map/pallas_call | solution.py:645
  97.8 0.8 copy.16

commit v4 on v3

--- a/solution.py
+++ b/solution.py
@@ -129,17 +129,17 @@
 
 
 def layer_kernel(
-    experts_n, columns, capacity, blocks,
+    experts_n, columns, capacity, widths,
     residual_hbm, value_hbm, gate_hbm, seg_hbm, conv_w_hbm, gain_hbm, shift_hbm, ow_hbm, ffn_hbm,
     routes_hbm, route_w_hbm, wg_hbm, wu_hbm, wd_hbm,
     out_ref,
     residual, value, gate, seg_ref, conv_w_ref, gain_ref, shift_ref, ow, ffn_ref, routes_ref, route_w_ref,
     wg, wu, wd, wg_in, wu_in, wd_in, rim, seg_in, seg_ext, ext, win, seg_win,
     conv_out, conv_in, stream, normed, outgoing, arrived, rows_in, relay_out, hidden, silu_gate, partial,
-    results, returned, relay_in, relay_sum, far_in, tables, picks, shares, routes_in, route_w_in,
+    results, returned, relay_in, relay_sum, far_in, help_in, pass_in, tables, picks, shares, routes_in, route_w_in,
     load_sem, y_send, y_recv, c_send, c_recv, f_send, f_recv, rim_send, rim_recv, x_send, x_recv,
     t_send, t_recv, far_send, far_recv, d_send, d_recv, e_recv, rd_send,
-    rb_send, rb_recv, r_send, r_recv, sum_send, sum_recv,
+    rb_send, rb_recv, r_send, r_recv, sum_send, sum_recv, h_send, h_recv, p_recv, q_send,
 ):
     me_s, me_t = lax.axis_index("sp"), lax.axis_index("tp")
     tok_dev, local = value.shape
@@ -148,7 +148,8 @@
     taps = conv_w_ref.shape[0]
     halves = normed.shape[0]
     half = width // halves
-    band = width // blocks
+    blocks = len(widths)
+    bands = [pl.ds(sum(widths[:j]), widths[j]) for j in range(blocks)]
     near_n = experts_n // 2
     near_slots = near_n * capacity
     next_s = (me_s + 1) % experts_n
@@ -178,6 +179,7 @@
     barrier = pltpu.get_barrier_semaphore()
     peers = [tp_peer(mask) for mask in range(1, columns)]
     peers += [sp_peer(mask) for mask in range(1, experts_n)]
+    peers.append((flipped(me_s, 2), flipped(me_t, 2)))
     for peer in peers:
         pl.semaphore_signal(barrier, inc=1, device_id=peer, device_id_type=MESH)
     for load in loads:
@@ -209,22 +211,39 @@
         )
 
     every, first_rows, second_rows = pl.ds(0, local), width // 8, width // 16
+    helped = help_in.shape[0] * help_in.shape[1]
     pieces = [
         (wg_hbm, wg_in, pl.ds(0, first_rows), every),
         (wg_hbm, wg_in, pl.ds(first_rows, second_rows), every),
         (wg_hbm, wg_in, pl.ds(first_rows + second_rows, width - first_rows - second_rows), every),
         (wu_hbm, wu_in, pl.ds(0, width // 2), every),
         (wu_hbm, wu_in, pl.ds(width // 2, width // 4), every),
-        (wu_hbm, wu_in, pl.ds(3 * width // 4, width // 4), every),
+        (wu_hbm, wu_in, pl.ds(3 * width // 4, width // 4 - helped), every),
+        (wu_hbm, wu_in, pl.ds(width - helped, helped), every),
     ]
     up_done = len(pieces)
-    pieces += [(wd_hbm, wd_in, every, pl.ds(j * band, band)) for j in range(blocks)]
+    detour = up_done - 1
+    pieces += [(wd_hbm, wd_in, every, bands[j]) for j in range(blocks)]
     across, forward = zip(*[across_piece(i, *piece) for i, piece in enumerate(pieces)])
     beside = [
         remote(own, into.at[0], c_send, c_recv.at[i], tp_peer(1))
         for i, (own, into) in enumerate(((wg_hbm, wg_in), (wu_hbm, wu_in), (wd_hbm, wd_in)))
     ]
     across[0].start()
+    parts = help_in.shape[0]
+
+    def helper(k, back):
+        rows = pl.ds(width - helped + k * (helped // parts), helped // parts)
+        if back:
+            return remote(help_in.at[k], wu_in.at[1, rows], h_send, y_recv.at[detour], sp_peer(2))
+        return remote(
+            wu_hbm.at[rows], help_in.at[k], y_send, h_recv.at[k], (flipped(me_s, 2), flipped(me_t, 2))
+        )
+
+    @pl.when(at_end)
+    def _():
+        for k in range(parts):
+            helper(k, False).start()
 
     relay = jnp.where(in_middle, flipped(me_s, 6), flipped(me_s, 4))
     relay_slot = jnp.where(in_middle, 0, 1)
@@ -295,7 +314,7 @@
         return [copy]
 
     conv_part(0)
-    across[1].start()
+    pl.when(at_end)(across[1].start)
 
     numbers = lax.broadcasted_iota(jnp.int32, (rows_own, lanes_n), 1).astype(jnp.float32)
     earlier = jnp.where(
@@ -331,8 +350,11 @@
     seg_ext[0:RIM, :] = jnp.where(me_s == 0, -1.0, before)
 
     conv_part(1)
-    for copy in across[2:]:
-        copy.start()
+    for i in range(1, len(pieces)):
+        if i == 1 or i == detour:
+            pl.when(in_middle)(across[i].start)
+        else:
+            across[i].start()
     conv_part(2)
     for copy in beside:
         copy.start()
@@ -350,9 +372,18 @@
                 lambda m: route_w_in[slot, m : m + 1, own_lanes],
             )
 
-    for i in range(2):
-        across[i].wait_recv()
-        forward[i].start()
+    @pl.when(in_middle)
+    def _():
+        for k in range(parts):
+            helper(k, False).wait_recv()
+            helper(k, True).start()
+
+    def pass_first():
+        for i in range(2):
+            across[i].wait_recv()
+            forward[i].start()
+
+    pl.when(at_end)(pass_first)
     for load in loads[conv_loads:stream_loads]:
         load.wait()
     swapped = remote(conv_in.at[pl.ds(1, columns - 1)], conv_in.at[pl.ds(1, columns - 1)], x_send, x_recv, tp_peer(1))
@@ -428,10 +459,18 @@
         load.wait()
     for copy in beside:
         copy.wait_recv()
+    relay_half(0, 0)
+    pl.when(in_middle)(pass_first)
     across[2].wait_recv()
     forward[2].start()
 
-    for h in range(halves):
+    def pass_detour():
+        across[detour].wait_recv()
+        forward[detour].start()
+
+    pl.when(at_end)(pass_detour)
+
+    for h in range(1, halves):
         relay_half(0, h)
 
     landed(others, d_recv)
@@ -480,6 +519,7 @@
 
     across[5].wait_recv()
     forward[5].start()
+    pl.when(in_middle)(pass_detour)
 
     def finish_hidden(mask):
         for rows in (near, far):
@@ -495,7 +535,7 @@
 
     def to_relay(mask, m, slot, j):
         return remote(
-            results.at[j, packet(mask)], relay_in.at[slot, j, packet(m)],
+            results.at[packet(mask), bands[j]], relay_in.at[slot, packet(m), bands[j]],
             rb_send, rb_recv.at[slot, j], sp_peer(m),
         )
 
@@ -504,14 +544,24 @@
     kept = ((6, 0), (4, 1))
     give_back = {
         (mask, j): remote(
-            results.at[j, packet(mask)], returned.at[j, packet(mask)],
+            results.at[packet(mask), bands[j]], returned.at[packet(mask), bands[j]],
             r_send, r_recv.at[j], sp_peer(mask),
         )
         for j in range(blocks) for mask in range(1, near_n)
     }
 
+    def pass_on(j):
+        return remote(
+            results.at[packet(3), bands[j]], pass_in.at[:, bands[j]], r_send, p_recv, sp_peer(1)
+        )
+
+    def passed(j):
+        return remote(
+            pass_in.at[:, bands[j]], returned.at[packet(3), bands[j]], q_send, r_recv.at[j], sp_peer(2)
+        )
+
     def band_results(j):
-        cols = slice(j * band, (j + 1) * band)
+        cols, span = bands[j], slice(0, widths[j])
         across[up_done + j].wait_recv()
         forward[up_done + j].start()
 
@@ -519,23 +569,25 @@
             w = wd[:, cols] if mask == 0 else wd_in[mask - 1, :, cols]
             return jnp.dot(hidden[mask], w, preferred_element_type=jnp.float32)
 
-        partial[...] = down(0) + down(1) + down(2)
+        partial[:, span] = down(0) + down(1) + down(2)
         forward[up_done + j].wait_recv()
-        results[j] = (partial[...] + down(3)).astype(jnp.bfloat16)
+        results[:, cols] = (partial[:, span] + down(3)).astype(jnp.bfloat16)
 
         @pl.when(in_middle)
         def _():
             for mask, m, slot in from_middle:
                 to_relay(mask, m, slot, j).start()
             for mask, slot in kept:
-                relay_in[slot, j, 0:capacity, :] = results[j, mask * capacity : (mask + 1) * capacity, :]
+                relay_in[slot, 0:capacity, cols] = results[mask * capacity : (mask + 1) * capacity, cols]
 
         @pl.when(at_end)
         def _():
             for mask, m, slot in from_end:
                 to_relay(mask, m, slot, j).start()
-
-        returned[j, 0:capacity, :] = results[j, 0:capacity, :]
+            pass_on(j).start()
+            give_back[1, j].start()
+
+        returned[0:capacity, cols] = results[0:capacity, cols]
 
     def direct(j, masks):
         for mask in masks:
@@ -543,7 +595,7 @@
 
     def summed_up(slot, j):
         return remote(
-            relay_sum.at[slot, j], far_in.at[j], sum_send, sum_recv.at[j],
+            relay_sum.at[slot, :, bands[j]], far_in.at[:, bands[j]], sum_send, sum_recv.at[j],
             sp_peer((6, 4)[slot]),
         )
 
@@ -558,36 +610,47 @@
         def _():
             for slot in range(2):
                 remote(
-                    relay_in.at[slot, j, others], relay_in.at[slot, j, others],
+                    relay_in.at[slot, others, bands[j]], relay_in.at[slot, others, bands[j]],
                     rb_send, rb_recv.at[slot, j], sp_peer(1),
                 ).wait_recv()
-                relay_sum[slot, j] = weighed(1 + slot, relay_in[slot, j]).astype(jnp.bfloat16)
+                relay_sum[slot, :, bands[j]] = weighed(1 + slot, relay_in[slot, :, bands[j]]).astype(jnp.bfloat16)
                 summed_up(slot, j).start()
 
-    early, lag = blocks // 4, blocks // 2
+    early, summed, ends = blocks // 4, 0, [sum(widths[: j + 1]) for j in range(blocks)]
     for j in range(blocks):
         band_results(j)
         pl.when(in_middle)(functools.partial(direct, j, (3, 2)))
         if j < early:
-            pl.when(at_end)(functools.partial(direct, j, (3, 2)))
-        if j >= lag:
-            relay_band(j - lag)
-    for j in range(blocks):
-        if j >= early:
-            pl.when(at_end)(functools.partial(direct, j, (3, 2)))
-        direct(j, (1,))
-    for j in range(blocks - lag, blocks):
+            pl.when(at_end)(functools.partial(direct, j, (2,)))
+        while ends[summed] + max(widths) <= ends[j]:
+            relay_band(summed)
+            summed += 1
+
+    @pl.when(in_middle)
+    def _():
+        for j in range(blocks):
+            direct(j, (1,))
+
+    @pl.when(at_end)
+    def _():
+        for j in range(early, blocks):
+            direct(j, (2,))
+        remote(pass_in, pass_in, r_send, p_recv, sp_peer(1)).wait_recv()
+        for j in range(blocks):
+            passed(j).start()
+
+    for j in range(summed, blocks):
         relay_band(j)
 
     def finish(j):
-        cols = slice(j * band, (j + 1) * band)
+        cols = bands[j]
         remote(
-            relay_sum.at[0, j], far_in.at[j], sum_send, sum_recv.at[j], (relay, me_t)
+            relay_sum.at[0, :, cols], far_in.at[:, cols], sum_send, sum_recv.at[j], (relay, me_t)
         ).wait_recv()
         remote(
-            returned.at[j, others], returned.at[j, others], r_send, r_recv.at[j], sp_peer(1)
+            returned.at[others, cols], returned.at[others, cols], r_send, r_recv.at[j], sp_peer(1)
         ).wait_recv()
-        total = stream[:, cols] + weighed(0, returned[j]) + far_in[j].astype(jnp.float32)
+        total = stream[:, cols] + weighed(0, returned[:, cols]) + far_in[:, cols].astype(jnp.float32)
         out_ref[:, cols] = total.astype(jnp.bfloat16)
 
     for j in range(blocks // 2):
@@ -604,17 +667,19 @@
         sent(wg_in, sem)
     swapped.wait_send()
     sent(outgoing.at[:, others], d_send)
-    sent(results.at[:, others], r_send)
+    sent(results.at[others, :], r_send)
 
     @pl.when(in_middle)
     def _():
         sent(relay_out.at[:, :, others], rd_send)
         sent(relay_sum, sum_send)
-        sent(results.at[:, pl.ds(0, 2 * capacity)], rb_send)
+        sent(results.at[pl.ds(0, 2 * capacity), :], rb_send)
+        sent(help_in, h_send)
 
     @pl.when(at_end)
     def _():
-        sent(results.at[:, pl.ds(0, 4 * capacity)], rb_send)
+        sent(results.at[pl.ds(0, 4 * capacity), :], rb_send)
+        sent(pass_in, q_send)
 
 
 def shards(*args):
@@ -631,8 +696,10 @@
     lanes = DC // CONV_GROUPS
     slot_total = experts_n * capacity
     near_slots = slot_total // 2
-    halves, blocks = 2, 8
-    half, band = width // halves, width // blocks
+    halves, fine = 2, width // 16
+    widths = (fine, fine) + (2 * fine,) * 6 + (fine, fine)
+    half, blocks = width // halves, len(widths)
+    helped = 4 * (width // 32)
     bf16, f32 = jnp.bfloat16, jnp.float32
     vmem, dma = pltpu.VMEM, pltpu.SemaphoreType.DMA
     anywhere = pl.BlockSpec(memory_space=pl.ANY)
@@ -643,7 +710,7 @@
         routes.T, route_weights.T, w_gate[0], w_up[0], w_down[0],
     )
     return pl.pallas_call(
-        functools.partial(layer_kernel, experts_n, columns, capacity, blocks),
+        functools.partial(layer_kernel, experts_n, columns, capacity, widths),
         out_shape=pltpu.VMEM((rows_own, width), bf16),
         in_specs=[anywhere] * len(operands),
         out_specs=pl.BlockSpec(memory_space=pltpu.VMEM),
@@ -657,18 +724,18 @@
             vmem((halves, near_slots, half), bf16), vmem((halves, slot_total, half), bf16),
             vmem((2, halves, rows_own, half), bf16), vmem((2, halves, near_slots, half), bf16),
             vmem((columns, slot_total, local), bf16), vmem((2, slot_total, local), f32),
-            vmem((slot_total, band), f32),
-            vmem((blocks, slot_total, band), bf16), vmem((blocks, near_slots, band), bf16),
-            vmem((2, blocks, near_slots, band), bf16), vmem((2, blocks, rows_own, band), bf16),
-            vmem((blocks, rows_own, band), bf16),
+            vmem((slot_total, 2 * fine), f32),
+            vmem((slot_total, width), bf16), vmem((near_slots, width), bf16),
+            vmem((2, near_slots, width), bf16), vmem((2, rows_own, width), bf16),
+            vmem((rows_own, width), bf16), vmem((2, helped // 2, local), bf16), vmem((capacity, width), bf16),
             vmem((3, top_count, rows_own, near_slots), bf16), vmem((3, near_slots, rows_own), bf16),
             vmem((3, top_count, rows_own, rows_own), f32),
             vmem((2, top_count, tok_dev), routes.dtype), vmem((2, top_count, tok_dev), route_weights.dtype),
-            dma((len(operands),)), dma, dma((6 + blocks,)), dma, dma((3,)),
-            dma, dma((6 + blocks,)), dma((3,)), dma((3,)), dma, dma,
+            dma((len(operands),)), dma, dma((7 + blocks,)), dma, dma((3,)),
+            dma, dma((7 + blocks,)), dma((3,)), dma((3,)), dma, dma,
             dma((2,)), dma((2, 2)), dma((halves,)), dma((2, halves)),
             dma, dma, dma, dma,
-            dma, dma((2, blocks)), dma, dma((blocks,)), dma, dma((blocks,)),
+            dma, dma((2, blocks)), dma, dma((blocks,)), dma, dma((blocks,)), dma, dma((2,)), dma, dma,
         ],
         compiler_params=pltpu.CompilerParams(
             collective_id=0, has_side_effects=True, vmem_limit_bytes=60 * 1024 * 1024

time: 98.7 us -> 95.8 us (0.971)
  Pallas kernels: 97.8 us -> 94.8 us
    pallas_call x1, Pallas kernels: 97.8 us -> 94.8 us  [shards(): pl.pallas_call(functools.partial(layer_kernel, experts_n, columns, capaci...]
where the time goes in v4:
time: 95.8 us; the launch traced here: 95.6 us
  Pallas kernels  94.8 us (99%)
    pallas_call x1, Pallas kernels, shards(): pl.pallas_call(functools.partial(layer_kernel, experts_n, columns, capaci...  94.8 us

profile of v4, /device:TPU:0, one launch (start us, length us, event | category | flops | bytes accessed | tf_op | source)
XLA Modules:
  0.0 95.6 jit_solution(14769139516983367297)
XLA Ops:
  0.0 94.8 %shard_map.136 = bf16[128,2048]{1,0:T(8,128)(2,1)S(1)} custom-call(bf16[128,2048]{1,0:T(8,128)(2,1)} %residual_hbm.1, bf16[512,256]{1,0:T(8,128)(2,1)} %value_hbm.1, bf16[512,256]{1,0:T(8,128)(2,1)} %gate_hbm.1, s32[4,128]{1,0:T(4,128)} %bitcast.15, f32[31,256]{1,0:T(8,128)} %conv_w_hbm.1, f32[1,256]{1,0:T(1,128)} %bitcast.16, f32[1,256]{1,0:T(1,128)} %bitcast.17, ...), custom_call_target="tpu_custom_call" | custom-call | tf_op jit(solution)/shard_map/pallas_call | solution.py:712
  94.8 0.8 copy.16

commit v5 on v4

--- a/solution.py
+++ b/solution.py
@@ -136,10 +136,10 @@
     residual, value, gate, seg_ref, conv_w_ref, gain_ref, shift_ref, ow, ffn_ref, routes_ref, route_w_ref,
     wg, wu, wd, wg_in, wu_in, wd_in, rim, seg_in, seg_ext, ext, win, seg_win,
     conv_out, conv_in, stream, normed, outgoing, arrived, rows_in, relay_out, hidden, silu_gate, partial,
-    results, returned, relay_in, relay_sum, far_in, help_in, pass_in, tables, picks, shares, routes_in, route_w_in,
+    results, returned, relay_in, relay_sum, far_in, help_in, pass_in, through_in, tables, picks, shares, routes_in, route_w_in,
     load_sem, y_send, y_recv, c_send, c_recv, f_send, f_recv, rim_send, rim_recv, x_send, x_recv,
     t_send, t_recv, far_send, far_recv, d_send, d_recv, e_recv, rd_send,
-    rb_send, rb_recv, r_send, r_recv, sum_send, sum_recv, h_send, h_recv, p_recv, q_send,
+    rb_send, rb_recv, r_send, r_recv, sum_send, sum_recv, h_send, h_recv, p_recv, q_send, v_recv,
 ):
     me_s, me_t = lax.axis_index("sp"), lax.axis_index("tp")
     tok_dev, local = value.shape
@@ -229,7 +229,8 @@
         remote(own, into.at[0], c_send, c_recv.at[i], tp_peer(1))
         for i, (own, into) in enumerate(((wg_hbm, wg_in), (wu_hbm, wu_in), (wd_hbm, wd_in)))
     ]
-    across[0].start()
+    pl.when(at_end)(across[0].start)
+    pl.when(in_middle)(across[1].start)
     parts = help_in.shape[0]
 
     def helper(k, back):
@@ -350,8 +351,8 @@
     seg_ext[0:RIM, :] = jnp.where(me_s == 0, -1.0, before)
 
     conv_part(1)
-    for i in range(1, len(pieces)):
-        if i == 1 or i == detour:
+    for i in (0, *range(2, len(pieces))):
+        if i == 0 or i == detour:
             pl.when(in_middle)(across[i].start)
         else:
             across[i].start()
@@ -497,6 +498,15 @@
     across[3].wait_recv()
     forward[3].start()
 
+    for i in range(3):
+        forward[i].wait_recv()
+
+    def gate_units(rows):
+        for mask in (2, 3):
+            silu_gate[mask - 2, rows, :] = silu(act(wg_in.at[mask - 1], rows))
+
+    gate_units(near)
+
     @pl.when(in_middle)
     def _():
         landed(pl.ds(near_slots, 2 * capacity), e_recv)
@@ -511,11 +521,7 @@
     across[4].wait_recv()
     forward[4].start()
 
-    for i in range(3):
-        forward[i].wait_recv()
-    for mask in (2, 3):
-        for rows in (near, far):
-            silu_gate[mask - 2, rows, :] = silu(act(wg_in.at[mask - 1], rows))
+    gate_units(far)
 
     across[5].wait_recv()
     forward[5].start()
@@ -531,6 +537,9 @@
     for i in range(3, up_done):
         forward[i].wait_recv()
 
+    across[up_done].wait_recv()
+    forward[up_done].start()
+
     finish_hidden(3)
 
     def to_relay(mask, m, slot, j):
@@ -540,7 +549,7 @@
         )
 
     from_middle = ((7, 1, 0), (5, 1, 1))
-    from_end = ((4, 2, 0), (6, 2, 1), (5, 3, 0), (7, 3, 1))
+    from_end, by_partner = ((4, 2, 0), (6, 2, 1), (7, 3, 1)), (5, 3, 0)
     kept = ((6, 0), (4, 1))
     give_back = {
         (mask, j): remote(
@@ -560,10 +569,25 @@
             pass_in.at[:, bands[j]], returned.at[packet(3), bands[j]], q_send, r_recv.at[j], sp_peer(2)
         )
 
+    def through(j):
+        return remote(
+            results.at[packet(by_partner[0]), bands[j]], through_in.at[:, bands[j]],
+            rb_send, v_recv.at[j], sp_peer(1),
+        )
+
+    def pass_through(j):
+        through(j).wait_recv()
+        _, m, slot = by_partner
+        remote(
+            through_in.at[:, bands[j]], relay_in.at[slot, packet(m), bands[j]],
+            q_send, rb_recv.at[slot, j], sp_peer(2),
+        ).start()
+
     def band_results(j):
         cols, span = bands[j], slice(0, widths[j])
-        across[up_done + j].wait_recv()
-        forward[up_done + j].start()
+        if j:
+            across[up_done + j].wait_recv()
+            forward[up_done + j].start()
 
         def down(mask):
             w = wd[:, cols] if mask == 0 else wd_in[mask - 1, :, cols]
@@ -582,6 +606,7 @@
 
         @pl.when(at_end)
         def _():
+            through(j).start()
             for mask, m, slot in from_end:
                 to_relay(mask, m, slot, j).start()
             pass_on(j).start()
@@ -616,9 +641,13 @@
                 relay_sum[slot, :, bands[j]] = weighed(1 + slot, relay_in[slot, :, bands[j]]).astype(jnp.bfloat16)
                 summed_up(slot, j).start()
 
-    early, summed, ends = blocks // 4, 0, [sum(widths[: j + 1]) for j in range(blocks)]
+    early, summed, ends = blocks // 2, 0, [sum(widths[: j + 1]) for j in range(blocks)]
+    forwarded = 0
     for j in range(blocks):
         band_results(j)
+        while ends[forwarded] + max(widths) <= ends[j]:
+            pl.when(at_end)(functools.partial(pass_through, forwarded))
+            forwarded += 1
         pl.when(in_middle)(functools.partial(direct, j, (3, 2)))
         if j < early:
             pl.when(at_end)(functools.partial(direct, j, (2,)))
@@ -633,6 +662,8 @@
 
     @pl.when(at_end)
     def _():
+        for j in range(forwarded, blocks):
+            pass_through(j)
         for j in range(early, blocks):
             direct(j, (2,))
         remote(pass_in, pass_in, r_send, p_recv, sp_peer(1)).wait_recv()
@@ -679,7 +710,7 @@
     @pl.when(at_end)
     def _():
         sent(results.at[pl.ds(0, 4 * capacity), :], rb_send)
-        sent(pass_in, q_send)
+        sent(results.at[pl.ds(0, 2 * capacity), :], q_send)
 
 
 def shards(*args):
@@ -728,6 +759,7 @@
             vmem((slot_total, width), bf16), vmem((near_slots, width), bf16),
             vmem((2, near_slots, width), bf16), vmem((2, rows_own, width), bf16),
             vmem((rows_own, width), bf16), vmem((2, helped // 2, local), bf16), vmem((capacity, width), bf16),
+            vmem((capacity, width), bf16),
             vmem((3, top_count, rows_own, near_slots), bf16), vmem((3, near_slots, rows_own), bf16),
             vmem((3, top_count, rows_own, rows_own), f32),
             vmem((2, top_count, tok_dev), routes.dtype), vmem((2, top_count, tok_dev), route_weights.dtype),
@@ -735,7 +767,7 @@
             dma, dma((7 + blocks,)), dma((3,)), dma((3,)), dma, dma,
             dma((2,)), dma((2, 2)), dma((halves,)), dma((2, halves)),
             dma, dma, dma, dma,
-            dma, dma((2, blocks)), dma, dma((blocks,)), dma, dma((blocks,)), dma, dma((2,)), dma, dma,
+            dma, dma((2, blocks)), dma, dma((blocks,)), dma, dma((blocks,)), dma, dma((2,)), dma, dma, dma((blocks,)),
         ],
         compiler_params=pltpu.CompilerParams(
             collective_id=0, has_side_effects=True, vmem_limit_bytes=60 * 1024 * 1024

time: 95.8 us -> 94.7 us (0.989)
  Pallas kernels: 94.8 us -> 93.8 us
    pallas_call x1, Pallas kernels: 94.8 us -> 93.8 us  [shards(): pl.pallas_call(functools.partial(layer_kernel, experts_n, columns, capaci...]
where the time goes in v5:
time: 94.7 us; the launch traced here: 94.6 us
  Pallas kernels  93.8 us (99%)
    pallas_call x1, Pallas kernels, shards(): pl.pallas_call(functools.partial(layer_kernel, experts_n, columns, capaci...  93.8 us

profile of v5, /device:TPU:0, one launch (start us, length us, event | category | flops | bytes accessed | tf_op | source)
XLA Modules:
  0.0 94.6 jit_solution(15197995727912160261)
XLA Ops:
  0.0 93.8 %shard_map.136 = bf16[128,2048]{1,0:T(8,128)(2,1)S(1)} custom-call(bf16[128,2048]{1,0:T(8,128)(2,1)} %residual_hbm.1, bf16[512,256]{1,0:T(8,128)(2,1)} %value_hbm.1, bf16[512,256]{1,0:T(8,128)(2,1)} %gate_hbm.1, s32[4,128]{1,0:T(4,128)} %bitcast.15, f32[31,256]{1,0:T(8,128)} %conv_w_hbm.1, f32[1,256]{1,0:T(1,128)} %bitcast.16, f32[1,256]{1,0:T(1,128)} %bitcast.17, ...), custom_call_target="tpu_custom_call" | custom-call | tf_op jit(solution)/shard_map/pallas_call | solution.py:743
  93.8 0.8 copy.16

commit v6 on v5

--- a/solution.py
+++ b/solution.py
@@ -633,7 +633,7 @@
     def relay_band(j):
         @pl.when(in_middle)
         def _():
-            for slot in range(2):
+            for slot in (1, 0):
                 remote(
                     relay_in.at[slot, others, bands[j]], relay_in.at[slot, others, bands[j]],
                     rb_send, rb_recv.at[slot, j], sp_peer(1),
@@ -649,6 +649,8 @@
             pl.when(at_end)(functools.partial(pass_through, forwarded))
             forwarded += 1
         pl.when(in_middle)(functools.partial(direct, j, (3, 2)))
+        if j >= 3:
+            pl.when(in_middle)(functools.partial(direct, j - 3, (1,)))
         if j < early:
             pl.when(at_end)(functools.partial(direct, j, (2,)))
         while ends[summed] + max(widths) <= ends[j]:
@@ -657,7 +659,7 @@
 
     @pl.when(in_middle)
     def _():
-        for j in range(blocks):
+        for j in range(blocks - 3, blocks):
             direct(j, (1,))
 
     @pl.when(at_end)

time: 94.7 us -> 94.9 us (level)
  no operation moved by 1% of the time
where the time goes in v6:
time: 94.9 us; the launch traced here: 94.7 us
  Pallas kernels  93.9 us (99%)
    pallas_call x1, Pallas kernels, shards(): pl.pallas_call(functools.partial(layer_kernel, experts_n, columns, capaci...  93.9 us

profile of v6, /device:TPU:0, one launch (start us, length us, event | category | flops | bytes accessed | tf_op | source)
XLA Modules:
  0.0 94.7 jit_solution(17255837735857163267)
XLA Ops:
  0.0 93.9 %shard_map.136 = bf16[128,2048]{1,0:T(8,128)(2,1)S(1)} custom-call(bf16[128,2048]{1,0:T(8,128)(2,1)} %residual_hbm.1, bf16[512,256]{1,0:T(8,128)(2,1)} %value_hbm.1, bf16[512,256]{1,0:T(8,128)(2,1)} %gate_hbm.1, s32[4,128]{1,0:T(4,128)} %bitcast.15, f32[31,256]{1,0:T(8,128)} %conv_w_hbm.1, f32[1,256]{1,0:T(1,128)} %bitcast.16, f32[1,256]{1,0:T(1,128)} %bitcast.17, ...), custom_call_target="tpu_custom_call" | custom-call | tf_op jit(solution)/shard_map/pallas_call | solution.py:745
  93.9 0.8 copy.16
